TPU v7x, 256 devices: a 4x2x16 block of a 4x16x16 slice. The times are simulated.
256 devices in a mesh: grp: 2 (over y), sp: 32 (over z, core), tp: 4 (over x).
Axes of the slice: x: 4, y: 2, z: 16, core: 2. Of those that a mesh axis runs over, the one named last changes fastest.
The devices are a block of a 4x16x16 slice.
Arguments:
- receptance: bfloat16 [8192, 512], P(('grp', 'sp'), 'tp'), parts along dimension 0, may hold values from -6 to 6
- key_matrix: bfloat16 [8192, 512], P(('grp', 'sp'), 'tp'), parts along dimension 0, may hold values from -6 to 6
- value_matrix: bfloat16 [8192, 512], P(('grp', 'sp'), 'tp'), parts along dimension 0, may hold values from -6 to 6
- output_gate_logits: bfloat16 [8192, 512], P(('grp', 'sp'), 'tp'), parts along dimension 0, may hold values from -6 to 6
- onward_decay_logits: bfloat16 [8192, 512], P(('grp', 'sp'), 'tp'), parts along dimension 0, may hold values from -14 to 3
- reverse_decay_logits: bfloat16 [8192, 512], P(('grp', 'sp'), 'tp'), parts along dimension 0, may hold values from -14 to 3
- correction_rate_logits: bfloat16 [8192, 512], P(('grp', 'sp'), 'tp'), parts along dimension 0, may hold values from -12 to 5
- extra_log_decay: float32 [8192, 8], P(('grp', 'sp'), 'tp'), parts along dimension 0, may hold values from -0.7 to 0
- documents: int32 [8192], P(('grp', 'sp')), parts along dimension 0, may hold values from 0 to 7, never falling along the last dimension, each value on 1 to 2048 neighbouring positions
- head_norm_scale: float32 [512], P('tp'), may hold values from 0.1 to 1.9
- mixer_output_weight: bfloat16 [512, 2048], P('tp'), may hold values from -0.25 to 0.25
- residual: bfloat16 [8192, 2048], P(('grp', 'sp', 'tp')), parts along dimension 0, may hold values from -6 to 6
- expert_norm_scale: float32 [2048], replicated, may hold values from 0.1 to 1.9
- expert_choice_index: int32 [8192, 2], P(('grp', 'sp', 'tp')), parts along dimension 0, may hold values from 0 to 127, as said below
- group_route_weight: float32 [8192], P(('grp', 'sp', 'tp')), parts along dimension 0, may hold values from 0.2 to 1
- expert_route_weight: float32 [8192, 2], P(('grp', 'sp', 'tp')), parts along dimension 0, may hold values from 0.05 to 1
- expert_gate_matrix: bfloat16 [128, 2048, 512], P(('sp', 'tp')), may hold values from -0.125 to 0.125
- expert_up_matrix: bfloat16 [128, 2048, 512], P(('sp', 'tp')), may hold values from -0.125 to 0.125
- expert_down_matrix: bfloat16 [128, 512, 2048], P(('sp', 'tp')), may hold values from -0.25 to 0.25
Outputs:
- updated: bfloat16 [8192, 2048], P(('grp', 'sp', 'tp')), parts along dimension 0
There are 2 independent parts, one for each index of `grp`. A program takes and returns all parts, laid end to end along the dimension named above; an argument that names none is the same for every part. Nothing has to cross between parts.
Inputs may be any that keep to these rules, and one draw needn't show every extreme that they name: `expert_choice_index`: each row names two different experts of one group (experts g * 4 to g * 4 + 3). In each aligned block of 32 rows no expert is named more than 2 times, and one expert is named exactly 2 times in every block.
All inputs are finite; a program needn't handle non-finite values.
Results may differ from a plain program's by a relative error of at most 0.012.
Values may be sent and summed in bfloat16 or wider, within the bound.
A program may use at most 64 MiB of HBM per device.

v0:
```python
import jax
import jax.numpy as jnp
from jax import lax
from jax.sharding import Mesh
from jax.sharding import PartitionSpec as P

HEAD_DIM = 64
SP = ("sp_0", "sp_1")
SP_TP = ("sp_0", "sp_1", "tp")
GRP_SP = ("grp", "sp_0", "sp_1")
GRP_SP_TP = ("grp", "sp_0", "sp_1", "tp")


longest_span = 128


def neutral_like(value, identity):
    return jax.tree.map(
        lambda part, zero: jnp.zeros_like(part) + jnp.asarray(zero, part.dtype), value, identity
    )


def gathered_once(value, axis):
    leaves = jax.tree.leaves(value)
    turns = sorted(range(len(leaves)), key=lambda k: -leaves[k].size)
    width = (1, *leaves[turns[0]].shape)[-1]
    lines = [
        jnp.pad(leaves[k].reshape(-1), (0, -leaves[k].size % width)).reshape(-1, width)
        for k in turns
    ]
    both, at, found = (lax.all_gather(jnp.concatenate(lines), axis), 0, {})
    for k, line in zip(turns, lines):
        slab = both[:, at : at + len(line)].reshape(len(both), -1)
        found[k] = slab[:, : leaves[k].size].reshape(-1, *leaves[k].shape)
        at += len(line)
    numbers = iter(range(len(leaves)))
    return jax.tree.map(lambda _: found[next(numbers)], value)


def prefix_by_axis(value, axes, combine, identity, reverse):
    before = start = neutral_like(value, identity)
    running = value
    for axis in reversed(axes):
        devices, position = (lax.axis_size(axis), lax.axis_index(axis))
        pieces = gathered_once(
            jax.tree.map(
                lambda part, kind: part.astype(kind),
                running,
                jax.tree.map(lambda a: jnp.bfloat16 if a.dtype == jnp.float32 else a.dtype, value),
            ),
            axis,
        )
        inside, running = (start, start)
        for k in reversed(range(devices)) if reverse else range(devices):
            passed = k > position if reverse else k < position
            running = combine(
                running, jax.tree.map(lambda part, own: part[k].astype(own.dtype), pieces, value)
            )
            inside = jax.tree.map(lambda new, old: jnp.where(passed, new, old), running, inside)
        before = combine(inside, before)
    return before


def in_blocks(value, dim, devices):
    before, after = (value.shape[:dim], value.shape[dim + 1 :])
    return jnp.moveaxis(value.reshape(*before, devices, -1, *after), dim, 0)


def summed_on_arrival(value, axis, dim):
    devices = lax.axis_size(axis)
    parts = lax.all_to_all(in_blocks(value, dim, devices), axis, 0, 0, tiled=True)
    return jnp.sum(parts.astype(jnp.float32), axis=0)


def into_blocks(array, count):
    length, heads, width = array.shape
    return array.reshape(count, length // count, heads, width).transpose(0, 2, 1, 3)


def from_blocks(array):
    count, heads, length, width = array.shape
    return array.transpose(0, 2, 1, 3).reshape(count * length, heads, width)


def block_step(state, item):
    reader, key_heads, unit_keys, rates, log_decay, block_docs, before_doc, values = item
    running = jnp.cumsum(log_decay, axis=1)
    probe = unit_keys * jnp.exp(running - log_decay)
    undo = jnp.exp(-running)
    fix_keys = rates * unit_keys * undo
    add_keys = key_heads * undo
    length = block_docs.shape[0]
    match = (block_docs[:, None] == block_docs[None, :]).astype(jnp.float32)
    strict = jnp.tril(jnp.ones((length, length), jnp.float32), -1) * match
    inclusive = jnp.tril(jnp.ones((length, length), jnp.float32)) * match
    opened = (block_docs == before_doc).astype(jnp.float32)[None, :, None]
    fix_mix = jnp.einsum("htn,hsn->hts", probe, fix_keys) * strict
    add_mix = jnp.einsum("htn,hsn->hts", probe, add_keys) * strict
    source = -opened * jnp.einsum("htn,hrn->htr", probe, state) - jnp.einsum(
        "hts,hsr->htr", add_mix, values
    )
    system = jnp.eye(length, dtype=jnp.float32)[None] + fix_mix
    removed = lax.linalg.triangular_solve(
        system, source, left_side=True, lower=True, unit_diagonal=True
    )
    closing = jnp.exp(running[:, -1:, :])
    tail_mask = match[-1][None, :, None]
    new_state = (
        opened[:, -1:, :] * state * closing
        + jnp.einsum("hsr,hsn->hrn", removed * tail_mask, fix_keys * closing)
        + jnp.einsum("hsr,hsn->hrn", values * tail_mask, add_keys * closing)
    )
    lifted = reader * jnp.exp(running)
    read_fix = jnp.einsum("htn,hsn->hts", lifted, fix_keys) * inclusive
    read_add = jnp.einsum("htn,hsn->hts", lifted, add_keys) * inclusive
    output = (
        opened * jnp.einsum("htn,hrn->htr", lifted, state)
        + jnp.einsum("hts,hsr->htr", read_fix, removed)
        + jnp.einsum("hts,hsr->htr", read_add, values)
    )
    return (new_state, output)


def device_pass(state, items):

    def advance(carry, item):
        return block_step(carry, item)

    return lax.scan(advance, state, items)


def chain(earlier, later):
    carry_map_a, carry_add_a, doc_head_a, doc_tail_a = earlier
    carry_map_b, carry_add_b, doc_head_b, doc_tail_b = later
    linked = jnp.logical_or(
        doc_tail_a == doc_head_b, jnp.logical_or(doc_tail_a < 0, doc_head_b < 0)
    ).astype(jnp.float32)
    carry_map = linked * jnp.einsum("hij,hjk->hik", carry_map_a, carry_map_b)
    carry_add = linked * jnp.einsum("hij,hjk->hik", carry_add_a, carry_map_b) + carry_add_b
    doc_head = jnp.where(doc_head_a < 0, doc_head_b, doc_head_a)
    doc_tail = jnp.where(doc_tail_b < 0, doc_tail_a, doc_tail_b)
    return (carry_map, carry_add, doc_head, doc_tail)


def oriented(reader, key_heads, unit_keys, rates, log_decay, doc_float):
    span_length = min(longest_span, reader.shape[0])
    count = reader.shape[0] // span_length
    block_docs = doc_float.reshape(count, span_length)
    before_doc = jnp.concatenate([block_docs[:1, 0], block_docs[:-1, -1]])
    return (
        (
            into_blocks(reader, count),
            into_blocks(key_heads, count),
            into_blocks(unit_keys, count),
            into_blocks(rates, count),
            into_blocks(log_decay, count),
            block_docs,
            before_doc,
        ),
        count,
    )


def local_pass(reader, key_heads, value_heads, unit_keys, rates, log_decay, doc_float):
    heads = reader.shape[1]
    blocks, count = oriented(reader, key_heads, unit_keys, rates, log_decay, doc_float)
    eye_heads = jnp.broadcast_to(jnp.eye(HEAD_DIM, dtype=jnp.float32), (heads, HEAD_DIM, HEAD_DIM))
    augmented = jnp.concatenate([jnp.zeros_like(eye_heads), eye_heads], axis=1)
    widened = into_blocks(
        jnp.concatenate([value_heads, jnp.zeros_like(value_heads)], axis=-1), count
    )
    final, outputs = device_pass(augmented, blocks + (widened,))
    element = (final[:, HEAD_DIM:], final[:, :HEAD_DIM], doc_float[0], doc_float[-1])
    return (blocks, into_blocks(value_heads, count), element, outputs)


def settle(carried, outputs, own_head):
    entry = carried[1] * (carried[3] == own_head).astype(jnp.float32)
    result = outputs[..., :HEAD_DIM] + jnp.einsum("hvk,bhck->bhcv", entry, outputs[..., HEAD_DIM:])
    return from_blocks(result)


def expert_rows(block, gate_local, up_local, down_local):
    shape = block.shape
    flat_rows = block.reshape(-1, shape[-1])
    activated = (
        jax.nn.silu(jnp.dot(flat_rows, gate_local, preferred_element_type=jnp.float32))
        * jnp.dot(flat_rows, up_local, preferred_element_type=jnp.float32)
    ).astype(jnp.bfloat16)
    return (
        jnp.dot(activated, down_local, preferred_element_type=jnp.float32)
        .astype(jnp.bfloat16)
        .reshape(shape)
    )


def body(
    receptance,
    key_matrix,
    value_matrix,
    output_gate_logits,
    onward_decay_logits,
    reverse_decay_logits,
    correction_rate_logits,
    extra_log_decay,
    documents,
    head_norm_scale,
    mixer_output_weight,
    residual,
    expert_norm_scale,
    expert_choice_index,
    group_route_weight,
    expert_route_weight,
    expert_gate_matrix,
    expert_up_matrix,
    expert_down_matrix,
):
    length, local_width = receptance.shape
    heads = local_width // HEAD_DIM
    triple_shape3 = (length, heads, HEAD_DIM)
    reader = receptance.astype(jnp.float32).reshape(triple_shape3)
    key_heads = key_matrix.astype(jnp.float32).reshape(triple_shape3)
    value_heads = value_matrix.astype(jnp.float32).reshape(triple_shape3)
    unit_keys = key_heads * lax.rsqrt(
        jnp.sum(key_heads * key_heads, axis=-1, keepdims=True) + 1e-06
    )
    rates = jax.nn.sigmoid(correction_rate_logits.astype(jnp.float32)).reshape(triple_shape3)
    decay_spike = extra_log_decay[:, :, None]
    onward_log_decay = (
        -jnp.exp(-jax.nn.softplus(-onward_decay_logits.astype(jnp.float32)) - 0.5).reshape(
            triple_shape3
        )
        + decay_spike
    )
    reverse_log_decay = (
        -jnp.exp(-jax.nn.softplus(-reverse_decay_logits.astype(jnp.float32)) - 0.5).reshape(
            triple_shape3
        )
        + decay_spike
    )
    doc_float = documents.astype(jnp.float32)
    blocks_fwd, values_fwd, element_fwd, outputs_fwd = local_pass(
        reader, key_heads, value_heads, unit_keys, rates, onward_log_decay, doc_float
    )
    blocks_bwd, values_bwd, element_bwd, outputs_bwd = local_pass(
        reader[::-1],
        key_heads[::-1],
        value_heads[::-1],
        unit_keys[::-1],
        rates[::-1],
        reverse_log_decay[::-1],
        doc_float[::-1],
    )
    eye_heads = jnp.broadcast_to(jnp.eye(HEAD_DIM, dtype=jnp.float32), (heads, HEAD_DIM, HEAD_DIM))
    neutral = (
        eye_heads,
        jnp.zeros_like(eye_heads),
        jnp.full((), -1.0, jnp.float32),
        jnp.full((), -1.0, jnp.float32),
    )
    carried_fwd = prefix_by_axis(element_fwd, SP, chain, neutral, False)
    carried_bwd = prefix_by_axis(element_bwd, SP, chain, neutral, True)
    forward = settle(carried_fwd, outputs_fwd, doc_float[0])
    backward = settle(carried_bwd, outputs_bwd, doc_float[-1])[::-1]
    total = forward + backward
    centred = total - jnp.mean(total, axis=-1, keepdims=True)
    scaled = centred * lax.rsqrt(jnp.mean(centred * centred, axis=-1, keepdims=True) + 0.00064)
    mix = (
        scaled.reshape(length, local_width)
        * head_norm_scale
        * jax.nn.sigmoid(output_gate_logits.astype(jnp.float32))
    ).astype(jnp.bfloat16)
    projected = summed_on_arrival(
        jnp.dot(mix, mixer_output_weight, preferred_element_type=jnp.float32).astype(jnp.bfloat16),
        "tp",
        0,
    )
    hidden = (residual.astype(jnp.float32) + projected).astype(jnp.bfloat16)
    hidden_f = hidden.astype(jnp.float32)
    normed = (
        hidden_f
        * lax.rsqrt(jnp.mean(hidden_f * hidden_f, axis=-1, keepdims=True) + 1e-06)
        * expert_norm_scale
    ).astype(jnp.bfloat16)
    count_rows, width = normed.shape
    size_sp = lax.axis_size(SP)
    size_tp = lax.axis_size("tp")
    experts = size_sp * size_tp
    capacity = max(2, 4 * count_rows // experts)
    flat_ids = expert_choice_index.reshape(-1)
    copies = flat_ids.shape[0]
    hits = (flat_ids[:, None] == jnp.arange(experts, dtype=jnp.int32)[None, :]).astype(jnp.float32)
    earlier_copies = jnp.tril(jnp.ones((copies, copies), jnp.float32), -1)
    ranks = jnp.sum(jnp.dot(earlier_copies, hits) * hits, axis=1).astype(jnp.int32)
    placed = flat_ids * capacity + ranks
    table = (jnp.arange(experts * capacity, dtype=jnp.int32)[:, None] == placed[None, :]).astype(
        jnp.bfloat16
    )
    pick_lead = table[:, 0::2]
    pick_trail = table[:, 1::2]
    outgoing = jnp.dot(pick_lead + pick_trail, normed, preferred_element_type=jnp.float32).astype(
        jnp.bfloat16
    )
    gate_local = expert_gate_matrix[0]
    up_local = expert_up_matrix[0]
    down_local = expert_down_matrix[0]
    returned = lax.all_to_all(
        expert_rows(
            lax.all_to_all(
                outgoing.reshape(experts, capacity, width),
                SP_TP,
                split_axis=0,
                concat_axis=0,
                tiled=True,
            ),
            gate_local,
            up_local,
            down_local,
        ),
        SP_TP,
        split_axis=0,
        concat_axis=0,
        tiled=True,
    )
    returned = returned.reshape(experts * capacity, width)
    answer_lead = jnp.einsum("sr,sd->rd", pick_lead, returned, preferred_element_type=jnp.float32)
    answer_trail = jnp.einsum("sr,sd->rd", pick_trail, returned, preferred_element_type=jnp.float32)
    weights = (
        group_route_weight[:, None]
        * expert_route_weight
        / jnp.sum(expert_route_weight, axis=-1, keepdims=True)
    )
    return (hidden_f + weights[:, :1] * answer_lead + weights[:, 1:] * answer_trail).astype(
        jnp.bfloat16
    )


def solution(mesh):
    split = Mesh(
        mesh.devices.reshape(mesh.shape["grp"], 16, 2, mesh.shape["tp"]),
        ("grp", "sp_0", "sp_1", "tp"),
    )
    in_specs = (
        P(GRP_SP, "tp"),
        P(GRP_SP, "tp"),
        P(GRP_SP, "tp"),
        P(GRP_SP, "tp"),
        P(GRP_SP, "tp"),
        P(GRP_SP, "tp"),
        P(GRP_SP, "tp"),
        P(GRP_SP, "tp"),
        P(GRP_SP),
        P("tp"),
        P("tp", None),
        P(GRP_SP_TP, None),
        P(),
        P(GRP_SP_TP, None),
        P(GRP_SP_TP),
        P(GRP_SP_TP, None),
        P(SP_TP, None, None),
        P(SP_TP, None, None),
        P(SP_TP, None, None),
    )
    out_specs = P(GRP_SP_TP, None)
    return jax.shard_map(body, mesh=split, in_specs=in_specs, out_specs=out_specs, check_vma=False)
```

profile of v0, /device:TPU:33, one launch (start us, length us, event | category | flops | bytes accessed | tf_op | source)
XLA Modules:
  0.0 561.0 jit_solution(8852569431941271812)
XLA Ops:
  13.8 21.1 %custom-call.5 = f32[2,1,128,128]{2,3,1,0:T(8,128)} custom-call(f32[2,1,128,128]{3,2,1,0:T(8,128)} %fusion.32), custom_call_target="InvertDiagBlocksLowerTriangular" | custom-call | tf_op jit(solution)/shard_map/while/body/eval_jaxpr/triangular_solve/custom-call.1 | solution.py:103
  40.7 1.5 convolution_add_fusion.4
  46.8 19.7 %custom-call.4 = f32[2,1,128,128]{2,3,1,0:T(8,128)S(1)} custom-call(f32[2,1,128,128]{3,2,1,0:T(8,128)S(1)} %fusion.21), custom_call_target="InvertDiagBlocksLowerTriangular" | custom-call | tf_op jit(solution)/shard_map/while/body/eval_jaxpr/triangular_solve/custom-call.1 | solution.py:103
  69.1 1.6 convolution_add_fusion.9
  74.2 21.9 %all-gather.4 = bf16[2,258,64]{1,2,0:T(8,128)(2,1)S(1)} all-gather(bf16[1,258,64]{1,2,0:T(8,128)(2,1)S(1)} %get-tuple-element.158), channel_id=2, replica_groups=mesh['grp'=2,'sp_0'=16,'sp_1'=2,'tp'=4] {'sp_1'}, dimensions={0}, use_global_device_ids=true | all-gather | bytes 99072 | tf_op jit(solution)/shard_map/all_gather | solution.py:31
  105.6 27.1 %all-gather.5 = bf16[16,258,64]{1,2,0:T(8,128)(2,1)S(1)} all-gather(bf16[1,258,64]{1,2,0:T(8,128)(2,1)S(1)} %maximum_bitcast_fusion.1), channel_id=3, replica_groups=mesh['grp'=2,'sp_0'=16,'sp_1'=2,'tp'=4] {'sp_0'}, dimensions={0}, use_global_device_ids=true | all-gather | bytes 561408 | tf_op jit(solution)/shard_map/all_gather | solution.py:31
  179.1 9.1 %all-gather.6 = bf16[2,258,64]{1,2,0:T(8,128)(2,1)S(1)} all-gather(bf16[1,258,64]{1,2,0:T(8,128)(2,1)} %get-tuple-element.159), channel_id=4, replica_groups=mesh['grp'=2,'sp_0'=16,'sp_1'=2,'tp'=4] {'sp_1'}, dimensions={0}, use_global_device_ids=true | all-gather | bytes 99072 | tf_op jit(solution)/shard_map/all_gather | solution.py:31
  198.1 23.9 %all-gather.7 = bf16[16,258,64]{1,2,0:T(8,128)(2,1)S(1)} all-gather(bf16[1,258,64]{1,2,0:T(8,128)(2,1)S(1)} %maximum_bitcast_fusion.3), channel_id=5, replica_groups=mesh['grp'=2,'sp_0'=16,'sp_1'=2,'tp'=4] {'sp_0'}, dimensions={0}, use_global_device_ids=true | all-gather | bytes 561408 | tf_op jit(solution)/shard_map/all_gather | solution.py:31
  222.9 1.7 copy.844
  224.6 1.6 fusion.254
  246.7 1.7 copy.845
  248.4 1.6 fusion.255
  270.8 1.5 copy.732
  273.4 1.9 fusion.28
  275.4 2.0 fusion.35
  279.0 1.5 reshape.1037
  281.9 1.5 reshape.1038
  284.8 1.5 reshape.1039
  287.7 1.5 reshape.1040
  290.6 1.5 reshape.1041
  293.5 1.5 reshape.1042
  296.4 1.5 reshape.1043
  299.3 1.5 reshape.1044
  302.2 1.5 reshape.1045
  305.1 1.5 reshape.1046
  308.0 1.5 reshape.1047
  310.9 1.5 reshape.1048
  313.8 1.5 reshape.1049
  316.7 1.5 reshape.1050
  326.3 1.5 reshape.1092
  329.2 1.5 reshape.1093
  332.1 1.5 reshape.1094
  335.0 1.5 reshape.1095
  337.9 1.5 reshape.1096
  340.8 1.5 reshape.1097
  343.7 1.5 reshape.1098
  349.4 1.5 reshape.1100
  352.3 1.5 reshape.1101
  355.2 1.5 reshape.1102
  398.7 4.3 all-to-all-start
  405.0 4.9 all-to-all-done
  410.6 1.5 reshape.991
  412.1 71.6 %all_to_all.15 = bf16[128,2,2048]{2,1,0:T(2,128)(2,1)S(1)} all-to-all(bf16[128,2,2048]{2,1,0:T(2,128)(2,1)} %reshape.991), channel_id=1, replica_groups=mesh['grp'=2,'sp_0'=16,'sp_1'=2,'tp'=4] {'sp_0','sp_1','tp'}, dimensions={0} | all-to-all | bytes 2097152 | tf_op jit(solution)/shard_map/all_to_all | solution.py:309
  485.0 3.5 fusion.6
  488.5 4.0 convolution_convert_fusion
  492.5 2.6 reshape.993
  495.1 8.5 %all-to-all-start.2 = ((bf16[128,2,2048]{2,1,0:T(2,128)(2,1)}), bf16[128,2,2048]{2,1,0:T(2,128)(2,1)}, u32[]{:S(2)}, u32[]{:S(2)}) async-start(bf16[128,2,2048]{2,1,0:T(2,128)(2,1)} %reshape.993), calls=%async_computation.2 | async-start | bytes 2097152 | tf_op jit(solution)/shard_map/all_to_all | solution.py:307
  506.2 52.0 %all-to-all-done.2 = bf16[128,2,2048]{2,1,0:T(2,128)(2,1)} async-done(((bf16[128,2,2048]{2,1,0:T(2,128)(2,1)}), bf16[128,2,2048]{2,1,0:T(2,128)(2,1)}, u32[]{:S(2)}, u32[]{:S(2)}) %all-to-all-start.2) | async-done | bytes 1048608 | tf_op jit(solution)/shard_map/all_to_all | solution.py:307
  (364 shorter events, 138.6 us)
Async XLA Ops:
  0.0 488.5 %copy-start = (bf16[1,512,2048]{2,1,0:T(8,128)(2,1)S(1)}, bf16[1,512,2048]{2,1,0:T(8,128)(2,1)}, u32[]{:S(2)}) copy-start(bf16[1,512,2048]{2,1,0:T(8,128)(2,1)} %param.39) | copy-start | bytes 6291460
  0.0 11.1 %copy-start.51 = (bf16[128,128]{1,0:T(8,128)(2,1)S(1)}, bf16[128,128]{1,0:T(8,128)(2,1)}, u32[]{:S(2)}) copy-start(bf16[128,128]{1,0:T(8,128)(2,1)} %param.27) | copy-start | bytes 98308
  5.1 37.1 %copy-start.1 = (f32[2,128,64]{1,2,0:T(8,128)}, f32[2,128,64]{1,2,0:T(8,128)S(1)}, u32[]{:S(2)}) copy-start(f32[2,128,64]{1,2,0:T(8,128)S(1)} %copy.638) | copy-start | bytes 196612
  9.9 33.6 %copy-start.10 = (f32[128,2,64]{0,2,1:T(8,128)}, f32[128,2,64]{0,2,1:T(8,128)S(1)}, u32[]{:S(2)}) copy-start(f32[128,2,64]{0,2,1:T(8,128)S(1)} %rev.29) | copy-start | bytes 196612
  10.5 35.7 %copy-start.2 = (f32[128,2,64]{2,0,1:T(8,128)}, f32[128,2,64]{2,0,1:T(8,128)S(1)}, u32[]{:S(2)}) copy-start(f32[128,2,64]{2,0,1:T(8,128)S(1)} %rev.30) | copy-start | bytes 196612
  12.9 33.9 %copy-start.6 = (f32[2,128,64]{1,2,0:T(8,128)}, f32[2,128,64]{1,2,0:T(8,128)S(1)}, u32[]{:S(2)}) copy-start(f32[2,128,64]{1,2,0:T(8,128)S(1)} %fusion.128) | copy-start | bytes 196612
  44.8 58.2 %copy-start.58 = (f32[128]{0:T(128)}, f32[128]{0:T(128)S(1)}, u32[]{:S(2)}) copy-start(f32[128]{0:T(128)S(1)} %get-tuple-element.66) | copy-start | bytes 1540
  46.2 57.4 %copy-start.7 = (f32[2,128,64]{1,2,0:T(8,128)}, f32[2,128,64]{1,2,0:T(8,128)S(1)}, u32[]{:S(2)}) copy-start(f32[2,128,64]{1,2,0:T(8,128)S(1)} %fusion.129) | copy-start | bytes 196612
  275.4 44.2 %copy-start.36 = (f32[1,128,64]{1,2,0:T(8,128)S(1)}, f32[1,128,64]{1,2,0:T(8,128)}, u32[]{:S(2)}) copy-start(f32[1,128,64]{1,2,0:T(8,128)} %get-tuple-element.70) | copy-start | bytes 98308
  277.3 44.4 %copy-start.35 = (f32[1,128,64]{1,2,0:T(8,128)S(1)}, f32[1,128,64]{1,2,0:T(8,128)}, u32[]{:S(2)}) copy-start(f32[1,128,64]{1,2,0:T(8,128)} %get-tuple-element.69) | copy-start | bytes 98308
  281.9 76.3 %copy-start.40 = (f32[1,128,64]{1,2,0:T(8,128)S(1)}, f32[1,128,64]{1,2,0:T(8,128)}, u32[]{:S(2)}) copy-start(f32[1,128,64]{1,2,0:T(8,128)} %get-tuple-element.121) | copy-start | bytes 98308
  284.8 75.5 %copy-start.39 = (f32[1,128,64]{1,2,0:T(8,128)S(1)}, f32[1,128,64]{1,2,0:T(8,128)}, u32[]{:S(2)}) copy-start(f32[1,128,64]{1,2,0:T(8,128)} %get-tuple-element.119) | copy-start | bytes 98308
  287.7 74.7 %copy-start.38 = (f32[1,128,64]{1,2,0:T(8,128)S(1)}, f32[1,128,64]{1,2,0:T(8,128)}, u32[]{:S(2)}) copy-start(f32[1,128,64]{1,2,0:T(8,128)} %get-tuple-element.117) | copy-start | bytes 98308
  290.6 74.0 %copy-start.37 = (f32[1,128,64]{1,2,0:T(8,128)S(1)}, f32[1,128,64]{1,2,0:T(8,128)}, u32[]{:S(2)}) copy-start(f32[1,128,64]{1,2,0:T(8,128)} %get-tuple-element.116) | copy-start | bytes 98308
  296.4 71.6 %copy-start.12 = (f32[2,128,128]{1,2,0:T(8,128)S(1)}, f32[2,128,128]{1,2,0:T(8,128)}, u32[]{:S(2)}) copy-start(f32[2,128,128]{1,2,0:T(8,128)} %fusion.28) | copy-start | bytes 393220
  296.4 71.6 %copy-start.14 = (f32[2,128,128]{1,2,0:T(8,128)S(1)}, f32[2,128,128]{1,2,0:T(8,128)}, u32[]{:S(2)}) copy-start(f32[2,128,128]{1,2,0:T(8,128)} %fusion.35) | copy-start | bytes 393220
  363.1 16.0 %copy-start.16 = (bf16[2,64,64]{1,2,0:T(8,128)(2,1)S(1)}, bf16[2,64,64]{1,2,0:T(8,128)(2,1)}, u32[]{:S(2)}) copy-start(bf16[2,64,64]{1,2,0:T(8,128)(2,1)} %copy-done.15) | copy-start | bytes 49156
  366.7 10.8 %copy-start.28 = (f32[2,64,64]{1,0,2:T(2,128)S(1)}, f32[2,64,64]{1,0,2:T(2,128)}, u32[]{:S(2)}) copy-start(f32[2,64,64]{1,0,2:T(2,128)} %reshape.1100) | copy-start | bytes 98308
  366.7 10.8 %copy-start.42 = (bf16[1,128,64]{2,1,0:T(8,128)(2,1)S(1)}, bf16[1,128,64]{2,1,0:T(8,128)(2,1)}, u32[]{:S(2)}) copy-start(bf16[1,128,64]{2,1,0:T(8,128)(2,1)} %copy.704) | copy-start | bytes 49156
  366.7 11.0 %copy-start.29 = (f32[2,64,64]{1,0,2:T(2,128)S(1)}, f32[2,64,64]{1,0,2:T(2,128)}, u32[]{:S(2)}) copy-start(f32[2,64,64]{1,0,2:T(2,128)} %reshape.1101) | copy-start | bytes 98308
  366.7 11.0 %copy-start.43 = (bf16[1,128,64]{2,1,0:T(8,128)(2,1)S(1)}, bf16[1,128,64]{2,1,0:T(8,128)(2,1)}, u32[]{:S(2)}) copy-start(bf16[1,128,64]{2,1,0:T(8,128)(2,1)} %copy.708) | copy-start | bytes 49156
  366.7 11.2 %copy-start.30 = (f32[2,64,64]{1,0,2:T(2,128)S(1)}, f32[2,64,64]{1,0,2:T(2,128)}, u32[]{:S(2)}) copy-start(f32[2,64,64]{1,0,2:T(2,128)} %reshape.1102) | copy-start | bytes 98308
  366.7 11.2 %copy-start.44 = (bf16[1,128,64]{2,1,0:T(8,128)(2,1)S(1)}, bf16[1,128,64]{2,1,0:T(8,128)(2,1)}, u32[]{:S(2)}) copy-start(bf16[1,128,64]{2,1,0:T(8,128)(2,1)} %copy.712) | copy-start | bytes 49156
  366.7 11.4 %copy-start.31 = (f32[2,64,64]{1,0,2:T(2,128)S(1)}, f32[2,64,64]{1,0,2:T(2,128)}, u32[]{:S(2)}) copy-start(f32[2,64,64]{1,0,2:T(2,128)} %reshape.1103) | copy-start | bytes 98308
  366.7 11.4 %copy-start.45 = (bf16[1,128,64]{2,1,0:T(8,128)(2,1)S(1)}, bf16[1,128,64]{2,1,0:T(8,128)(2,1)}, u32[]{:S(2)}) copy-start(bf16[1,128,64]{2,1,0:T(8,128)(2,1)} %copy.716) | copy-start | bytes 49156
  366.8 11.7 %copy-start.32 = (f32[2,64,64]{1,0,2:T(2,128)S(1)}, f32[2,64,64]{1,0,2:T(2,128)}, u32[]{:S(2)}) copy-start(f32[2,64,64]{1,0,2:T(2,128)} %reshape.1104) | copy-start | bytes 98308
  366.8 11.7 %copy-start.46 = (bf16[1,128,64]{2,1,0:T(8,128)(2,1)S(1)}, bf16[1,128,64]{2,1,0:T(8,128)(2,1)}, u32[]{:S(2)}) copy-start(bf16[1,128,64]{2,1,0:T(8,128)(2,1)} %copy.720) | copy-start | bytes 49156
  366.8 11.9 %copy-start.33 = (f32[2,64,64]{1,0,2:T(2,128)S(1)}, f32[2,64,64]{1,0,2:T(2,128)}, u32[]{:S(2)}) copy-start(f32[2,64,64]{1,0,2:T(2,128)} %reshape.1105) | copy-start | bytes 98308
  366.8 11.9 %copy-start.47 = (bf16[1,128,64]{2,1,0:T(8,128)(2,1)S(1)}, bf16[1,128,64]{2,1,0:T(8,128)(2,1)}, u32[]{:S(2)}) copy-start(bf16[1,128,64]{2,1,0:T(8,128)(2,1)} %copy.724) | copy-start | bytes 49156
  366.8 12.1 %copy-start.49 = (f32[2,64,64]{1,0,2:T(2,128)S(1)}, f32[2,64,64]{1,0,2:T(2,128)}, u32[]{:S(2)}) copy-start(f32[2,64,64]{1,0,2:T(2,128)} %reshape.1106) | copy-start | bytes 98308
  366.8 12.1 %copy-start.53 = (bf16[1,128,64]{2,1,0:T(8,128)(2,1)S(1)}, bf16[1,128,64]{2,1,0:T(8,128)(2,1)}, u32[]{:S(2)}) copy-start(bf16[1,128,64]{2,1,0:T(8,128)(2,1)} %copy.728) | copy-start | bytes 49156
  366.8 12.7 %copy-start.18 = (bf16[2,64,64]{1,2,0:T(8,128)(2,1)S(1)}, bf16[2,64,64]{1,2,0:T(8,128)(2,1)}, u32[]{:S(2)}) copy-start(bf16[2,64,64]{1,2,0:T(8,128)(2,1)} %copy-done.17) | copy-start | bytes 49156
  366.8 12.7 %copy-start.22 = (bf16[2,64,64]{1,2,0:T(8,128)(2,1)S(1)}, bf16[2,64,64]{1,2,0:T(8,128)(2,1)}, u32[]{:S(2)}) copy-start(bf16[2,64,64]{1,2,0:T(8,128)(2,1)} %copy-done.21) | copy-start | bytes 49156
  368.9 11.0 %copy-start.27 = (f32[2,64,64]{1,0,2:T(2,128)S(1)}, f32[2,64,64]{1,0,2:T(2,128)}, u32[]{:S(2)}) copy-start(f32[2,64,64]{1,0,2:T(2,128)} %reshape.1037) | copy-start | bytes 98308
  368.9 11.0 %copy-start.48 = (bf16[1,128,64]{2,1,0:T(8,128)(2,1)S(1)}, bf16[1,128,64]{2,1,0:T(8,128)(2,1)}, u32[]{:S(2)}) copy-start(bf16[1,128,64]{2,1,0:T(8,128)(2,1)} %copy.563) | copy-start | bytes 49156
  368.9 11.2 %copy-start.59 = (f32[128]{0:T(128)S(1)}, f32[128]{0:T(128)}, u32[]{:S(2)}) copy-start(f32[128]{0:T(128)} %copy-done.58) | copy-start | bytes 1540
  379.8 16.8 %copy-start.41 = (bf16[2,64,64]{1,2,0:T(8,128)(2,1)S(1)}, bf16[2,64,64]{1,2,0:T(8,128)(2,1)}, u32[]{:S(2)}) copy-start(bf16[2,64,64]{1,2,0:T(8,128)(2,1)} %copy.627) | copy-start | bytes 49156
  379.9 17.1 %copy-start.24 = (bf16[2,64,64]{1,2,0:T(8,128)(2,1)S(1)}, bf16[2,64,64]{1,2,0:T(8,128)(2,1)}, u32[]{:S(2)}) copy-start(bf16[2,64,64]{1,2,0:T(8,128)(2,1)} %copy-done.23) | copy-start | bytes 49156
  379.9 17.1 %copy-start.26 = (bf16[2,64,64]{1,2,0:T(8,128)(2,1)S(1)}, bf16[2,64,64]{1,2,0:T(8,128)(2,1)}, u32[]{:S(2)}) copy-start(bf16[2,64,64]{1,2,0:T(8,128)(2,1)} %copy-done.25) | copy-start | bytes 49156
  380.4 17.1 %copy-start.13 = (bf16[128,2048]{1,0:T(8,128)(2,1)S(1)}, bf16[128,2048]{1,0:T(8,128)(2,1)}, u32[]{:S(2)}) copy-start(bf16[128,2048]{1,0:T(8,128)(2,1)} %param.31) | copy-start | bytes 1572868
  380.5 17.1 %copy-start.52 = (bf16[128,128]{1,0:T(8,128)(2,1)S(1)}, bf16[128,128]{1,0:T(8,128)(2,1)}, u32[]{:S(2)}) copy-start(bf16[128,128]{1,0:T(8,128)(2,1)} %param.24) | copy-start | bytes 98308
  380.5 17.1 %copy-start.61 = (f32[128]{0:T(128)S(1)}, f32[128]{0:T(128)}, u32[]{:S(2)}) copy-start(f32[128]{0:T(128)} %param.30) | copy-start | bytes 1540
  397.0 13.0 %copy-start.34 = (bf16[32,2048]{1,0:T(8,128)(2,1)S(1)}, bf16[32,2048]{1,0:T(8,128)(2,1)}, u32[]{:S(2)}) copy-start(bf16[32,2048]{1,0:T(8,128)(2,1)} %param.32) | copy-start | bytes 393220
  397.4 12.7 %copy-start.56 = (f32[2048]{0:T(1024)S(1)}, f32[2048]{0:T(1024)}, u32[]{:S(2)}) copy-start(f32[2048]{0:T(1024)} %param.33) | copy-start | bytes 24580
  398.7 11.2 %all-to-all-start = ((bf16[4,32,2048]{2,1,0:T(8,128)(2,1)}), bf16[4,32,2048]{2,1,0:T(8,128)(2,1)S(1)}, u32[]{:S(2)}, u32[]{:S(2)}) async-start(bf16[4,32,2048]{2,1,0:T(8,128)(2,1)} %bitcast.237), calls=%async_computation | async-start | bytes 1048576 | tf_op jit(solution)/shard_map/all_to_all | solution.py:71
  492.5 13.7 %copy-start.57 = (f32[32,2]{0,1:T(2,128)S(1)}, f32[32,2]{0,1:T(2,128)}, u32[]{:S(2)}) copy-start(f32[32,2]{0,1:T(2,128)} %param.36) | copy-start | bytes 772
  492.5 13.7 %copy-start.62 = (f32[32]{0:T(128)S(1)}, f32[32]{0:T(128)}, u32[]{:S(2)}) copy-start(f32[32]{0:T(128)} %param.35) | copy-start | bytes 388
  495.1 63.1 %all-to-all-start.2 = ((bf16[128,2,2048]{2,1,0:T(2,128)(2,1)}), bf16[128,2,2048]{2,1,0:T(2,128)(2,1)}, u32[]{:S(2)}, u32[]{:S(2)}) async-start(bf16[128,2,2048]{2,1,0:T(2,128)(2,1)} %reshape.993), calls=%async_computation.2 | async-start | bytes 2097152 | tf_op jit(solution)/shard_map/all_to_all | solution.py:307
  (17 other events, 73.2 us)
where the time goes:
time: 568 us; the launch traced here: 561 us
  blocking collectives  154 us (27%)
  local copies, waits for them, and re-layouts  126 us (22%)
  between operations  96.1 us (17%)
  other arithmetic  58.3 us (10%)
  matrix products  57.1 us (10%)
  waiting for transfers between devices  56.8 us (10%)
  starting transfers between devices  12.8 us (2%)
    all_gather x4, blocking collectives, gathered_once(): both, at, found = (lax.all_gather(jnp.concatenate(lines), axis), 0, {})  82 us
    all_to_all x1, blocking collectives, body(): lax.all_to_all(outgoing.reshape(experts, capacity, width), SP_TP, split_a...  71.6 us
    all_to_all x1, waiting for transfers between devices, body(): lax.all_to_all(expert_rows(lax.all_to_all(outgoing.reshape(experts, capac...  52 us
    slice x40, local copies, waits for them, and re-layouts, prefix_by_axis(): part[k].astype(own.dtype)  51.6 us
    convert_element_type x36, local copies, waits for them, and re-layouts, prefix_by_axis(): part[k].astype(own.dtype)  42.4 us
    another operation x3, other arithmetic, block_step(): lax.linalg.triangular_solve(system, source, left_side=True, lower=True, u...  40.9 us
    dot_general x38, matrix products, chain(): jnp.einsum('hij,hjk->hik', carry_add_a, carry_map_b)  28.7 us
  transfers between devices with their start and end apart: 2, of which 2 were waited for; matrix products, arithmetic and copies ran while one was open for 1% of the time, Pallas kernels for 0%

commit v1 on v0

v1 whole, which is shorter than its diff:
```python
import functools

import jax
import jax.numpy as jnp
from jax import lax
from jax.experimental import pallas as pl
from jax.experimental.pallas import tpu as pltpu
from jax.sharding import PartitionSpec as P

HEAD_DIM = 64
GRP_SP = ("grp", "sp")
GRP_SP_TP = ("grp", "sp", "tp")
SP_TP = ("sp", "tp")
MESH = pl.DeviceIdType.MESH
HIGHEST = lax.Precision.HIGHEST
F32 = jnp.float32
BF16 = jnp.bfloat16
QUARTERS = 4
SLOTS = 4
GROUP = 4
CAP = 2
REACH = 4


def dot(a, b, dims=((1,), (0,)), precision=None):
    return lax.dot_general(a, b, (dims, ((), ())), preferred_element_type=F32, precision=precision)


def low(a, b, dims=((1,), (0,))):
    return dot(a.astype(BF16), b.astype(BF16), dims)


ROWS = ((0,), (0,))
LANES = ((1,), (1,))


def iota(shape, dim):
    return lax.broadcasted_iota(jnp.int32, shape, dim)


def sigmoid(x):
    return 1.0 / (1.0 + jnp.exp(-x))


def inverse(lower, row, col):
    eye = (row == col).astype(F32)
    near = jnp.where((row >> 3) == (col >> 3), lower, 0.0)
    second = dot(near, near, precision=HIGHEST)
    fourth = dot(second, second, precision=HIGHEST)
    found = dot(eye - near, eye + second, precision=HIGHEST)
    found = dot(found, eye + fourth, precision=HIGHEST)
    bit = 3
    while (1 << bit) < lower.shape[0]:
        across = ((row >> (bit + 1)) == (col >> (bit + 1))) & ((row >> bit) != (col >> bit))
        found = found - low(low(found, jnp.where(across, lower, 0.0)), found)
        bit += 1
    return found


def column_of(line, eye):
    return jnp.sum(jnp.where(eye, line, jnp.zeros_like(line)), axis=1, keepdims=True)


def line_of(column, eye):
    return jnp.sum(jnp.where(eye, column, jnp.zeros_like(column)), axis=0, keepdims=True)


def direction(reader, keys, values, unit, rates, log_decay, doc_col, doc_row, back):
    n = reader.shape[0]
    row, col = iota((n, n), 0), iota((n, n), 1)
    lane = iota((1, n), 1)
    first_head = lane < HEAD_DIM
    same_head = (row < HEAD_DIM) == (col < HEAD_DIM)
    upto = (col >= row) if back else (col <= row)
    match = doc_col == doc_row
    inclusive = upto & match
    strict = inclusive & (row != col)
    running = dot(upto.astype(F32), log_decay, precision=HIGHEST)
    total = running[:1] if back else running[n - 1 :]
    middle = 0.5 * total
    before = running - log_decay
    head_doc = doc_row[:, n - 1 :] if back else doc_row[:, :1]
    tail_doc = doc_row[:, :1] if back else doc_row[:, n - 1 :]
    opened = (doc_col == head_doc).astype(F32)
    closing = (doc_col == tail_doc).astype(F32)
    probe = unit * jnp.exp(before - middle)
    lifted = reader * jnp.exp(running - middle)
    undo = jnp.exp(middle - running)
    fix_keys = rates * unit * undo
    add_keys = keys * undo
    rest = jnp.exp(total - running)
    fix_last = rates * unit * rest
    add_last = keys * rest
    probe_open = opened * unit * jnp.exp(before)
    lifted_open = opened * reader * jnp.exp(running)
    left = jnp.concatenate([probe, lifted], axis=0)
    right = jnp.concatenate([fix_keys, add_keys], axis=0).astype(BF16)
    values_low = values.astype(BF16)
    removed, added, reads = [], [], []
    for head in range(2):
        mine = first_head if head == 0 else jnp.logical_not(first_head)
        grams = low(jnp.where(mine, left, 0.0), right, LANES)
        system = jnp.where(strict, grams[:n, :n], 0.0)
        add_mix = jnp.where(strict, grams[:n, n:], 0.0)
        reads.append(jnp.where(inclusive, grams[n:, :n], 0.0))
        read_add = jnp.where(inclusive, grams[n:, n:], 0.0)
        mixed = low(jnp.concatenate([add_mix, read_add], axis=0), values_low)
        added.append(mixed[n:])
        source = -jnp.concatenate([mixed[:n], probe_open], axis=1)
        removed.append(low(inverse(system, row, col), source))
    both = jnp.concatenate([first_head, first_head], axis=1)
    took = jnp.where(both, removed[0], removed[1])
    heads = [low(reads[head], took) for head in range(2)]
    through = jnp.where(both, heads[0], heads[1])
    outputs = through[:, :n] + jnp.where(first_head, added[0], added[1])
    response = through[:, n:] + lifted_open
    ends = low(took * closing, fix_last, ROWS)
    add = ends[:n] + low(values * closing, add_last, ROWS)
    whole = (head_doc == tail_doc).astype(F32)
    keep = ends[n:] + jnp.where(row == col, whole * jnp.exp(total), 0.0)
    add = jnp.where(same_head, add, 0.0)
    keep = jnp.where(same_head, keep, 0.0)
    half = n // 2
    element = jnp.concatenate(
        [
            keep[:half] + keep[half:],
            add[:half] + add[half:],
            jnp.broadcast_to(head_doc, (8, n)),
            jnp.broadcast_to(tail_doc, (8, n)),
        ],
        axis=0,
    ).astype(BF16)
    return outputs, response, element


def spread(block, same_head):
    return jnp.where(same_head, jnp.concatenate([block, block], axis=0), jnp.zeros_like(same_head, block.dtype))


def link(tail, head):
    return (tail == head).astype(F32)


def kernel(sizes, *refs):
    (
        receptance_ref, key_ref, value_ref, out_gate_ref, onward_ref, reverse_ref, rate_ref, extra_ref,
        docs_ref, head_scale_ref, mixer_hbm, residual_ref, expert_scale_ref, choice_ref, group_weight_ref,
        route_ref, gate_hbm, up_hbm, down_hbm,
        updated_ref,
        element, partner, chip, near, window, far, entering,
        partial, shares, meta_out, meta_in, packed, arrived, pick, weigh_hi, weigh_lo,
        outward, inbound, answers, answered, combined, returned,
        mixer_w, gate_w, up_w, down_w,
        w_sem, pair_sem, near_send, near_recv, far_sem, tp_send, tp_recv,
        meta_send, meta_recv, out_send, out_recv, x_send, x_recv, y_send, y_recv, back_send, back_recv,
    ) = refs
    SP, TP = sizes
    chips = SP // 2
    sp, tp = lax.axis_index("sp"), lax.axis_index("tp")
    z, core = lax.div(sp, 2), lax.rem(sp, 2)
    n = receptance_ref.shape[0]
    count, width = residual_ref.shape
    quarter = width // QUARTERS
    piece = QUARTERS * SLOTS

    barrier = pltpu.get_barrier_semaphore()

    def greet_sp(o, carry):
        pl.semaphore_signal(barrier, inc=1, device_id={"sp": lax.rem(sp + o, SP)}, device_id_type=MESH)
        return carry

    lax.fori_loop(1, SP, greet_sp, 0)
    for o in range(1, TP):
        pl.semaphore_signal(barrier, inc=1, device_id={"tp": lax.rem(tp + o, TP)}, device_id_type=MESH)

    loads = [
        pltpu.make_async_copy(src, dst, w_sem.at[k])
        for k, (src, dst) in enumerate(
            ((mixer_hbm, mixer_w), (gate_hbm, gate_w), (up_hbm, up_w), (down_hbm, down_w))
        )
    ]
    for load in loads:
        load.start()

    lane32, row32 = iota((count, count), 1), iota((count, count), 0)
    eye32 = lane32 == row32
    choice = choice_ref[...].astype(F32)
    lead, trail = choice[:, :1], choice[:, 1:2]
    lead_group = jnp.floor(lead * (1.0 / GROUP))
    lead_line, trail_line, group_line = (line_of(part, eye32) for part in (lead, trail, lead_group))
    earlier = lane32 < row32

    def rank(mask):
        return jnp.sum(jnp.where(earlier & mask, 1.0, 0.0), axis=1, keepdims=True)

    slot = rank(lead_group == group_line)
    lead_rank = rank((lead == lead_line) | (lead == trail_line))
    trail_rank = rank((trail == lead_line) | (trail == trail_line))
    route = route_ref[...]
    scale = column_of(group_weight_ref[...], eye32) / (route[:, :1] + route[:, 1:2])
    lane = iota((count, 128), 1).astype(F32)
    lead_own, trail_own = lead - GROUP * lead_group, trail - GROUP * lead_group
    info = (
        jnp.where(lane == lead_own, lead_rank + 1.0, 0.0)
        + jnp.where(lane == trail_own, trail_rank + 1.0, 0.0)
        + jnp.where(lane == lead_own + GROUP, scale * route[:, :1], 0.0)
        + jnp.where(lane == trail_own + GROUP, scale * route[:, 1:2], 0.0)
    )
    meta_lane = iota((count, SP * 8), 1)
    meta_pick = (lead_group == (meta_lane >> 3).astype(F32)) & (slot == (meta_lane & 7).astype(F32))
    meta_out[...] = dot(meta_pick.astype(F32).T, info, precision=HIGHEST)
    stacked = QUARTERS * count
    group4, slot4 = jnp.concatenate([lead_group] * QUARTERS, 0), jnp.concatenate([slot] * QUARTERS, 0)
    place = iota((stacked, SP * piece), 1)
    place_row = iota((stacked, SP * piece), 0)
    table_rows = (
        (group4 == (place >> 4).astype(F32))
        & (slot4 == (place & 3).astype(F32))
        & (lax.div(place_row, count) == ((place >> 2) & 3))
    ).astype(F32)

    pl.semaphore_wait(barrier, SP - 1 + TP - 1)

    def sp_copy(src, dst, send, recv, o, rows):
        peer = lax.rem(sp + o, SP)
        return pltpu.make_async_remote_copy(
            src_ref=src.at[pl.ds(pl.multiple_of(peer * rows, rows), rows)],
            dst_ref=dst.at[pl.ds(pl.multiple_of(sp * rows, rows), rows)],
            send_sem=send.at[o],
            recv_sem=recv.at[o],
            device_id={"sp": peer},
            device_id_type=MESH,
        )

    def turn(k):
        half = lax.div(k + 1, 2)
        return SP // 2 + jnp.where(lax.rem(k, 2) == 1, -half, half)

    def start_sp(src, dst, send, recv, rows):
        def one(k, carry):
            sp_copy(src, dst, send, recv, turn(k), rows).start()
            return carry

        lax.fori_loop(0, SP - 1, one, 0)

    def wait_sp(src, dst, send, recv, rows, which):
        def one(o, carry):
            copy = sp_copy(src, dst, send, recv, o, rows)
            copy.wait_send() if which == "send" else copy.wait_recv()
            return carry

        lax.fori_loop(1, SP, one, 0)

    def tp_copy(src, dst, send, recv, o, toward):
        peer = lax.rem(tp + (o if toward else TP - o), TP)
        return pltpu.make_async_remote_copy(
            src_ref=src, dst_ref=dst, send_sem=send.at[o], recv_sem=recv.at[o],
            device_id={"tp": peer}, device_id_type=MESH,
        )

    start_sp(meta_out, meta_in, meta_send, meta_recv, 8)

    row, col = iota((n, n), 0), iota((n, n), 1)
    eye = row == col
    same_head = (row < HEAD_DIM) == (col < HEAD_DIM)
    first_head = iota((1, n), 1) < HEAD_DIM
    doc_row = docs_ref[...].astype(F32)
    doc_col = column_of(doc_row, eye)
    reader = receptance_ref[...].astype(F32)
    keys = key_ref[...].astype(F32)
    values = value_ref[...].astype(F32)

    def by_head(x):
        one = jnp.sum(jnp.where(first_head, x, 0.0), axis=1, keepdims=True)
        two = jnp.sum(jnp.where(first_head, 0.0, x), axis=1, keepdims=True)
        return jnp.where(first_head, one, two)

    unit = keys * lax.rsqrt(by_head(keys * keys) + 1e-06)
    rates = sigmoid(rate_ref[...].astype(F32))
    extra = jnp.where(first_head, extra_ref[:, :1], extra_ref[:, 1:2])
    level = 0.6065306597126334
    onward = -level * sigmoid(onward_ref[...].astype(F32)) + extra
    reverse = -level * sigmoid(reverse_ref[...].astype(F32)) + extra
    out_f, resp_f, element_f = direction(reader, keys, values, unit, rates, onward, doc_col, doc_row, False)
    out_b, resp_b, element_b = direction(reader, keys, values, unit, rates, reverse, doc_col, doc_row, True)
    element[0] = element_f
    element[1] = element_b

    sign = 1 - 2 * core

    def pair_copy(src, dst, k):
        return pltpu.make_async_remote_copy(
            src_ref=src, dst_ref=dst, send_sem=pair_sem.at[2 * k], recv_sem=pair_sem.at[2 * k + 1],
            device_id={"sp": sp + sign}, device_id_type=MESH,
        )

    def chip_peer(distance):
        return lax.rem(z + sign * distance + chips, chips) * 2 + core

    def exists(distance):
        origin = z - sign * distance
        return (origin >= 0) & (origin < chips)

    half = n // 2

    def parts(ref_value):
        value = ref_value.astype(F32)
        return value[:half], value[half : 2 * half], value[n : n + 1], value[n + 8 : n + 9]

    first_copy = pair_copy(element.at[1 - core], partner, 0)
    first_copy.start()
    first_copy.wait()
    own = element[core].astype(F32)
    own_keep, own_add, own_head, own_tail = own[:half], own[half:n], own[n : n + 1], own[n + 8 : n + 9]
    par_keep, par_add, par_head, par_tail = parts(partner[...])
    joined = link(own_tail, par_head)
    both = joined * low(own[:n], spread(par_keep, same_head))
    chip[...] = jnp.concatenate(
        [both[:half], both[half:] + par_add, jnp.broadcast_to(own_head, (8, n)), jnp.broadcast_to(par_tail, (8, n))],
        axis=0,
    ).astype(BF16)

    def near_copy(k):
        return pltpu.make_async_remote_copy(
            src_ref=chip, dst_ref=near.at[k - 1], send_sem=near_send.at[k - 1], recv_sem=near_recv.at[k - 1],
            device_id={"sp": chip_peer(k)}, device_id_type=MESH,
        )

    for k in range(REACH, 0, -1):
        near_copy(k).start()
    for k in range(1, REACH + 1):
        near_copy(k).wait_recv()
    keep, add, win_head, tail = parts(near[REACH - 1])
    tail = jnp.where(exists(REACH), tail, -1.0)
    for k in range(REACH - 1, 0, -1):
        next_keep, next_add, next_head, next_tail = parts(near[k - 1])
        step = link(tail, next_head) * low(
            jnp.concatenate([keep, add], axis=0), spread(next_keep, same_head)
        )
        keep, add = step[:half], step[half:] + next_add
        tail = jnp.where(exists(k), next_tail, -1.0)
    window[...] = jnp.concatenate(
        [add, jnp.broadcast_to(tail, (16, n))], axis=0
    ).astype(BF16)
    far_copy = pltpu.make_async_remote_copy(
        src_ref=window, dst_ref=far, send_sem=far_sem.at[0], recv_sem=far_sem.at[1],
        device_id={"sp": chip_peer(REACH)}, device_id_type=MESH,
    )
    far_copy.start()
    for k in range(1, REACH + 1):
        near_copy(k).wait_send()
    far_copy.wait()
    far_value = far[...].astype(F32)
    far_tail = jnp.where(exists(REACH), far_value[half : half + 1], -1.0)
    add = add + link(far_tail, win_head) * low(far_value[:half], spread(keep, same_head))
    state = link(tail, own_head) * add
    passed = (low(state, spread(own_keep, same_head)) + own_add) * joined
    entering[0] = passed.astype(BF16)
    last_copy = pair_copy(entering.at[0], entering.at[1], 1)
    last_copy.start()
    last_copy.wait()
    other = entering[1].astype(F32)
    state_f = jnp.where(core == 0, state, other)
    state_b = jnp.where(core == 0, other, state)
    entry = jnp.concatenate([spread(state_f, same_head), spread(state_b, same_head)], axis=1)
    mixed = out_f + out_b + low(jnp.concatenate([resp_f, resp_b], axis=1), entry, LANES)

    centred = mixed - by_head(mixed) * (1.0 / HEAD_DIM)
    scaled = centred * lax.rsqrt(by_head(centred * centred) * (1.0 / HEAD_DIM) + 0.00064)
    mix = (scaled * head_scale_ref[...] * sigmoid(out_gate_ref[...].astype(F32))).astype(BF16)
    loads[0].wait()
    partial[...] = dot(mix, mixer_w[...]).astype(BF16)

    def share_copy(o):
        peer = lax.rem(tp + o, TP)
        src = partial.at[pl.ds(pl.multiple_of(peer * count, count), count)]
        return tp_copy(src, shares.at[o], tp_send, tp_recv, o, True)

    for o in (2, 1, 3):
        share_copy(o).start()
    hidden = residual_ref[...].astype(F32)
    own_share = partial[pl.ds(pl.multiple_of(tp * count, count), count)].astype(F32)
    for o in (1, 3, 2):
        share_copy(o).wait_recv()
    shared = own_share + shares[1].astype(F32) + shares[2].astype(F32) + shares[3].astype(F32)
    hidden = (hidden + shared).astype(BF16).astype(F32)
    normed = (
        hidden * lax.rsqrt(jnp.mean(hidden * hidden, axis=1, keepdims=True) + 1e-06) * expert_scale_ref[...]
    ).astype(BF16)

    quarters = jnp.concatenate([normed[:, q * quarter : (q + 1) * quarter] for q in range(QUARTERS)], axis=0)
    packed[...] = dot(table_rows.T.astype(BF16), quarters).astype(BF16)
    start_sp(packed, arrived, out_send, out_recv, piece)
    mine = pl.ds(pl.multiple_of(sp * piece, piece), piece)
    arrived[mine] = packed[mine]

    wait_sp(meta_out, meta_in, meta_send, meta_recv, 8, "recv")
    own_meta = pl.ds(pl.multiple_of(sp * 8, 8), 8)
    meta_in[own_meta] = meta_out[own_meta]
    size = SP * piece
    wide_row, wide_col = iota((size, SP * 8), 0), iota((size, SP * 8), 1)
    widen = ((wide_row >> 4) == (wide_col >> 3)) & ((wide_row & 3) == (wide_col & 7))
    meta = dot(widen.astype(F32), meta_in[...], precision=HIGHEST)
    meta_lane = iota((size, 128), 1)
    taken = SP * CAP
    t_row, t_col = iota((size, taken), 0), iota((size, taken), 1)
    same_source = (t_row >> 4) == (t_col >> 1)
    for o in range(TP):
        expert = lax.rem(tp + o, TP)
        code = jnp.sum(jnp.where(meta_lane == expert, meta, 0.0), axis=1, keepdims=True)
        weight = jnp.sum(jnp.where(meta_lane == expert + GROUP, meta, 0.0), axis=1, keepdims=True)
        hit = same_source & (code == ((t_col & 1) + 1).astype(F32))
        for q in range(QUARTERS):
            here = jnp.where(hit & (((t_row >> 2) & 3) == q), 1.0, 0.0)
            pick[o, q * taken : (q + 1) * taken] = here.T.astype(BF16)
            value = here * weight
            high = value.astype(BF16)
            at = slice((q * TP + o) * taken, (q * TP + o + 1) * taken)
            weigh_hi[o, q] = high
            weigh_lo[o, q] = (value - high.astype(F32)).astype(BF16)
    wait_sp(packed, arrived, out_send, out_recv, piece, "recv")

    def to_expert(o):
        return tp_copy(outward.at[o], inbound.at[o], x_send, x_recv, o, True)

    for o in (2, 1, 3, 0):
        rows = dot(pick[o], arrived[...]).astype(BF16)
        target = inbound if o == 0 else outward
        for q in range(QUARTERS):
            target[o, :, q * quarter : (q + 1) * quarter] = rows[q * taken : (q + 1) * taken]
        if o:
            to_expert(o).start()
    for load in loads[1:]:
        load.wait()
    for o in (1, 3, 2):
        to_expert(o).wait_recv()

    def back_copy(o):
        return tp_copy(answers.at[o], answered.at[o], y_send, y_recv, o, False)

    rows = inbound[...].reshape(TP * taken, width)
    gate = dot(rows, gate_w[...])
    up = dot(rows, up_w[...])
    active = (gate * sigmoid(gate) * up).astype(BF16)
    result = dot(active, down_w[...]).astype(BF16)
    for o in (2, 1, 3, 0):
        target = answered if o == 0 else answers
        target[o] = result[o * taken : (o + 1) * taken]
        if o:
            back_copy(o).start()
    for o in (1, 3, 2):
        back_copy(o).wait_recv()

    total = jnp.zeros((size, quarter), F32)
    for o in range(TP):
        for q in range(QUARTERS):
            answer = answered[o, :, q * quarter : (q + 1) * quarter]
            total += dot(weigh_hi[o, q], answer) + dot(weigh_lo[o, q], answer)
    combined[...] = total.astype(BF16)
    start_sp(combined, returned, back_send, back_recv, piece)
    returned[mine] = combined[mine]
    wait_sp(combined, returned, back_send, back_recv, piece, "recv")
    final = dot(table_rows.astype(BF16), returned[...])
    for q in range(QUARTERS):
        at = slice(q * quarter, (q + 1) * quarter)
        updated_ref[:, at] = (hidden[:, at] + final[q * count : (q + 1) * count]).astype(BF16)

    for o in range(1, TP):
        share_copy(o).wait_send()
        to_expert(o).wait_send()
        back_copy(o).wait_send()
    wait_sp(meta_out, meta_in, meta_send, meta_recv, 8, "send")
    wait_sp(packed, arrived, out_send, out_recv, piece, "send")
    wait_sp(combined, returned, back_send, back_recv, piece, "send")


def solution(mesh):
    SP, TP = mesh.shape["sp"], mesh.shape["tp"]

    def body(
        receptance, key_matrix, value_matrix, output_gate_logits, onward_decay_logits, reverse_decay_logits,
        correction_rate_logits, extra_log_decay, documents, head_norm_scale, mixer_output_weight, residual,
        expert_norm_scale, expert_choice_index, group_route_weight, expert_route_weight,
        expert_gate_matrix, expert_up_matrix, expert_down_matrix,
    ):
        n, channels = receptance.shape
        count, width = residual.shape
        hidden_units = expert_gate_matrix.shape[2]
        piece = QUARTERS * SLOTS
        size, taken, quarter = SP * piece, SP * CAP, width // QUARTERS
        vmem, hbm = pl.BlockSpec(memory_space=pltpu.VMEM), pl.BlockSpec(memory_space=pl.ANY)
        dma = pltpu.SemaphoreType.DMA
        return pl.pallas_call(
            functools.partial(kernel, (SP, TP)),
            out_shape=jax.ShapeDtypeStruct((count, width), BF16),
            in_specs=[vmem] * 10 + [hbm] + [vmem] * 5 + [hbm] * 3,
            out_specs=vmem,
            scratch_shapes=[
                pltpu.VMEM((2, n + 16, n), BF16),
                pltpu.VMEM((n + 16, n), BF16),
                pltpu.VMEM((n + 16, n), BF16),
                pltpu.VMEM((REACH, n + 16, n), BF16),
                pltpu.VMEM((n // 2 + 16, n), BF16),
                pltpu.VMEM((n // 2 + 16, n), BF16),
                pltpu.VMEM((2, n // 2, n), BF16),
                pltpu.VMEM((n, width), BF16),
                pltpu.VMEM((TP, count, width), BF16),
                pltpu.VMEM((SP * 8, 128), F32),
                pltpu.VMEM((SP * 8, 128), F32),
                pltpu.VMEM((size, quarter), BF16),
                pltpu.VMEM((size, quarter), BF16),
                pltpu.VMEM((TP, QUARTERS * taken, size), BF16),
                pltpu.VMEM((TP, QUARTERS, size, taken), BF16),
                pltpu.VMEM((TP, QUARTERS, size, taken), BF16),
                pltpu.VMEM((TP, taken, width), BF16),
                pltpu.VMEM((TP, taken, width), BF16),
                pltpu.VMEM((TP, taken, width), BF16),
                pltpu.VMEM((TP, taken, width), BF16),
                pltpu.VMEM((size, quarter), BF16),
                pltpu.VMEM((size, quarter), BF16),
                pltpu.VMEM((channels, width), BF16),
                pltpu.VMEM((width, hidden_units), BF16),
                pltpu.VMEM((width, hidden_units), BF16),
                pltpu.VMEM((hidden_units, width), BF16),
                dma((4,)), dma((4,)), dma((REACH,)), dma((REACH,)), dma((2,)), dma((TP,)), dma((TP,)),
                dma((SP,)), dma((SP,)), dma((SP,)), dma((SP,)), dma((TP,)), dma((TP,)), dma((TP,)), dma((TP,)),
                dma((SP,)), dma((SP,)),
            ],
            compiler_params=pltpu.CompilerParams(
                collective_id=0, has_side_effects=True, vmem_limit_bytes=56 * 1024 * 1024
            ),
        )(
            receptance, key_matrix, value_matrix, output_gate_logits, onward_decay_logits, reverse_decay_logits,
            correction_rate_logits, extra_log_decay, documents.reshape(1, n), head_norm_scale.reshape(1, channels),
            mixer_output_weight, residual, expert_norm_scale.reshape(1, width), expert_choice_index,
            group_route_weight.reshape(1, count), expert_route_weight,
            expert_gate_matrix[0], expert_up_matrix[0], expert_down_matrix[0],
        )

    in_specs = (
        (P(GRP_SP, "tp"),) * 8
        + (P(GRP_SP), P("tp"), P("tp", None), P(GRP_SP_TP, None), P(), P(GRP_SP_TP, None))
        + (P(GRP_SP_TP), P(GRP_SP_TP, None))
        + (P(SP_TP, None, None),) * 3
    )
    return jax.shard_map(
        body, mesh=mesh, in_specs=in_specs, out_specs=P(GRP_SP_TP, None), check_vma=False
    )
```

time: 568 us -> 153 us (0.27); the launches traced: 561 us -> 153 us
  blocking collectives: 154 us -> 0 us
  Pallas kernels: 0 us -> 147 us
  local copies, waits for them, and re-layouts: 126 us -> 5.69 us
  between operations: 96.1 us -> 0.01 us
  other arithmetic: 58.3 us -> 0 us
  matrix products: 57.1 us -> 0 us
  waiting for transfers between devices: 56.8 us -> 0 us
  starting transfers between devices: 12.8 us -> 0 us
    pallas_call x0 -> x1, Pallas kernels: none -> 147 us  [body(): pl.pallas_call(functools.partial(kernel, (SP, TP)), out_shape=jax.ShapeDt...]
    all_gather x4 -> x0, blocking collectives: 82 us -> none  [gathered_once(): both, at, found = (lax.all_gather(jnp.concatenate(lines), axis), 0, {})]
    all_to_all x1 -> x0, blocking collectives: 71.6 us -> none  [body(): lax.all_to_all(outgoing.reshape(experts, capacity, width), SP_TP, split_a...]
    slice x57 -> x0, local copies, waits for them, and re-layouts: 60.6 us -> none  [the longest x40 51.6 us: prefix_by_axis(): part[k].astype(own.dtype)]
    all_to_all x2 -> x0, waiting for transfers between devices: 56.8 us -> none  [the longest x1 52 us: body(): lax.all_to_all(expert_rows(lax.all_to_all(outgoing.reshape(experts, capac...]
    dot_general x67 -> x0, matrix products: 55.4 us -> none  [the longest x38 28.7 us: chain(): jnp.einsum('hij,hjk->hik', carry_add_a, carry_map_b)]
    convert_element_type x41 -> x0, local copies, waits for them, and re-layouts: 42.7 us -> none  [the longest x36 42.4 us: prefix_by_axis(): part[k].astype(own.dtype)]
    another operation x5 -> x0, other arithmetic: 41.2 us -> none  [the longest x3 40.9 us: block_step(): lax.linalg.triangular_solve(system, source, left_side=True, lower=True, u...]
  transfers between devices with their start and end apart: 2 -> 0, of which waited for: 2 -> 0; matrix products, arithmetic and copies ran while one was open for 1% -> 0% of each run, Pallas kernels for 0% -> 0%
where the time goes in v1:
time: 153 us
  Pallas kernels  147 us (96%)
  local copies, waits for them, and re-layouts  5.69 us (4%)
    pallas_call x1, Pallas kernels, body(): pl.pallas_call(functools.partial(kernel, (SP, TP)), out_shape=jax.ShapeDt...  147 us
    unnamed x4, local copies, waits for them, and re-layouts  5.69 us

profile of v1, /device:TPU:33, one launch (start us, length us, event | category | flops | bytes accessed | tf_op | source)
XLA Modules:
  0.0 153.2 jit_solution(15227939803021267768)
XLA Ops:
  0.0 1.4 copy.21.refs_13_
  1.4 1.4 copy.22.refs_15_
  2.7 1.4 copy.20.refs_7_
  4.1 147.5 %shard_map.181 = bf16[32,2048]{1,0:T(8,128)(2,1)} custom-call(bf16[128,128]{1,0:T(8,128)(2,1)} %refs_0_.1, bf16[128,128]{1,0:T(8,128)(2,1)} %refs_1_.1, bf16[128,128]{1,0:T(8,128)(2,1)} %refs_2_.1, bf16[128,128]{1,0:T(8,128)(2,1)} %refs_3_.1, bf16[128,128]{1,0:T(8,128)(2,1)} %refs_4_.1, bf16[128,128]{1,0:T(8,128)(2,1)} %refs_5_.1, bf16[128,128]{1,0:T(8,128)(2,1)} %refs_6_.1, ...), custom_call_target="tpu_custom_call" | custom-call | tf_op jit(solution)/shard_map/pallas_call | solution.py:493
  151.6 1.6 %copy.24 = bf16[32,2048]{1,0:T(8,128)(2,1)} copy(bf16[32,2048]{1,0:T(8,128)(2,1)} %shard_map.181) | data formatting | bytes 262144

commit v2 on v1

--- a/solution.py
+++ b/solution.py
@@ -19,6 +19,7 @@
 SLOTS = 4
 GROUP = 4
 CAP = 2
+CHUNKS = 4
 REACH = 4
 
 
@@ -148,11 +149,12 @@
         route_ref, gate_hbm, up_hbm, down_hbm,
         updated_ref,
         element, partner, chip, near, window, far, entering,
-        partial, shares, meta_out, meta_in, packed, arrived, pick, weigh_hi, weigh_lo,
+        mix_out, mixes, meta_out, meta_in, place, packed, arrived, pick, weigh_hi, weigh_lo,
         outward, inbound, answers, answered, combined, returned,
         mixer_w, gate_w, up_w, down_w,
-        w_sem, pair_sem, near_send, near_recv, far_sem, tp_send, tp_recv,
-        meta_send, meta_recv, out_send, out_recv, x_send, x_recv, y_send, y_recv, back_send, back_recv,
+        w_sem, pair_sem, near_send, near_recv, far_sem, mixer_send, mixer_recv, share_send, share_recv,
+        mix_send, mix_recv, meta_send, meta_recv, out_send, out_recv, x_send, x_recv, y_send, y_recv,
+        back_send, back_recv,
     ) = refs
     SP, TP = sizes
     chips = SP // 2
@@ -162,6 +164,10 @@
     count, width = residual_ref.shape
     quarter = width // QUARTERS
     piece = QUARTERS * SLOTS
+    size = SP * piece
+    group_slots = SP // CHUNKS
+    chunk = group_slots * piece
+    taken = group_slots * CAP
 
     barrier = pltpu.get_barrier_semaphore()
 
@@ -176,89 +182,66 @@
     loads = [
         pltpu.make_async_copy(src, dst, w_sem.at[k])
         for k, (src, dst) in enumerate(
-            ((mixer_hbm, mixer_w), (gate_hbm, gate_w), (up_hbm, up_w), (down_hbm, down_w))
+            ((mixer_hbm, mixer_w.at[tp]), (gate_hbm, gate_w), (up_hbm, up_w), (down_hbm, down_w))
         )
     ]
     for load in loads:
         load.start()
 
-    lane32, row32 = iota((count, count), 1), iota((count, count), 0)
-    eye32 = lane32 == row32
-    choice = choice_ref[...].astype(F32)
-    lead, trail = choice[:, :1], choice[:, 1:2]
-    lead_group = jnp.floor(lead * (1.0 / GROUP))
-    lead_line, trail_line, group_line = (line_of(part, eye32) for part in (lead, trail, lead_group))
-    earlier = lane32 < row32
-
-    def rank(mask):
-        return jnp.sum(jnp.where(earlier & mask, 1.0, 0.0), axis=1, keepdims=True)
-
-    slot = rank(lead_group == group_line)
-    lead_rank = rank((lead == lead_line) | (lead == trail_line))
-    trail_rank = rank((trail == lead_line) | (trail == trail_line))
-    route = route_ref[...]
-    scale = column_of(group_weight_ref[...], eye32) / (route[:, :1] + route[:, 1:2])
-    lane = iota((count, 128), 1).astype(F32)
-    lead_own, trail_own = lead - GROUP * lead_group, trail - GROUP * lead_group
-    info = (
-        jnp.where(lane == lead_own, lead_rank + 1.0, 0.0)
-        + jnp.where(lane == trail_own, trail_rank + 1.0, 0.0)
-        + jnp.where(lane == lead_own + GROUP, scale * route[:, :1], 0.0)
-        + jnp.where(lane == trail_own + GROUP, scale * route[:, 1:2], 0.0)
-    )
-    meta_lane = iota((count, SP * 8), 1)
-    meta_pick = (lead_group == (meta_lane >> 3).astype(F32)) & (slot == (meta_lane & 7).astype(F32))
-    meta_out[...] = dot(meta_pick.astype(F32).T, info, precision=HIGHEST)
-    stacked = QUARTERS * count
-    group4, slot4 = jnp.concatenate([lead_group] * QUARTERS, 0), jnp.concatenate([slot] * QUARTERS, 0)
-    place = iota((stacked, SP * piece), 1)
-    place_row = iota((stacked, SP * piece), 0)
-    table_rows = (
-        (group4 == (place >> 4).astype(F32))
-        & (slot4 == (place & 3).astype(F32))
-        & (lax.div(place_row, count) == ((place >> 2) & 3))
-    ).astype(F32)
-
-    pl.semaphore_wait(barrier, SP - 1 + TP - 1)
-
-    def sp_copy(src, dst, send, recv, o, rows):
-        peer = lax.rem(sp + o, SP)
+    def turn(k):
+        half = (k + 1) >> 1
+        return SP // 2 + jnp.where((k & 1) == 1, -half, half)
+
+    def ahead(k):
+        peer = sp + turn(k)
+        return jnp.where(peer >= SP, peer - SP, peer)
+
+    def behind(k):
+        peer = sp - turn(k)
+        return jnp.where(peer < 0, peer + SP, peer)
+
+    def sp_copy(src, dst, send, recv, k, back=False):
         return pltpu.make_async_remote_copy(
-            src_ref=src.at[pl.ds(pl.multiple_of(peer * rows, rows), rows)],
-            dst_ref=dst.at[pl.ds(pl.multiple_of(sp * rows, rows), rows)],
-            send_sem=send.at[o],
-            recv_sem=recv.at[o],
-            device_id={"sp": peer},
-            device_id_type=MESH,
-        )
-
-    def turn(k):
-        half = lax.div(k + 1, 2)
-        return SP // 2 + jnp.where(lax.rem(k, 2) == 1, -half, half)
-
-    def start_sp(src, dst, send, recv, rows):
+            src_ref=src, dst_ref=dst, send_sem=send.at[k], recv_sem=recv.at[k],
+            device_id={"sp": behind(k) if back else ahead(k)}, device_id_type=MESH,
+        )
+
+    def rows_at(ref, k):
+        return ref.at[pl.ds(pl.multiple_of(k * piece, piece), piece)]
+
+    def meta_copy(k):
+        return sp_copy(meta_out.at[k], meta_in.at[k], meta_send, meta_recv, k)
+
+    def out_copy(k):
+        return sp_copy(rows_at(packed, k), rows_at(arrived, k), out_send, out_recv, k)
+
+    def home_copy(k):
+        return sp_copy(rows_at(combined, k), rows_at(returned, k), back_send, back_recv, k, True)
+
+    def each(make, act, first=0, last=SP - 1):
         def one(k, carry):
-            sp_copy(src, dst, send, recv, turn(k), rows).start()
+            act(make(k))
             return carry
 
-        lax.fori_loop(0, SP - 1, one, 0)
-
-    def wait_sp(src, dst, send, recv, rows, which):
-        def one(o, carry):
-            copy = sp_copy(src, dst, send, recv, o, rows)
-            copy.wait_send() if which == "send" else copy.wait_recv()
-            return carry
-
-        lax.fori_loop(1, SP, one, 0)
-
-    def tp_copy(src, dst, send, recv, o, toward):
-        peer = lax.rem(tp + (o if toward else TP - o), TP)
+        lax.fori_loop(first, last, one, 0)
+
+    def begin(copy):
+        copy.start()
+
+    def leave(copy):
+        copy.wait_send()
+
+    def arrive(copy):
+        copy.wait_recv()
+
+    def bounds(c):
+        return c * group_slots, min((c + 1) * group_slots, SP - 1)
+
+    def tp_copy(src, dst, send, recv, k, o):
         return pltpu.make_async_remote_copy(
-            src_ref=src, dst_ref=dst, send_sem=send.at[o], recv_sem=recv.at[o],
-            device_id={"tp": peer}, device_id_type=MESH,
-        )
-
-    start_sp(meta_out, meta_in, meta_send, meta_recv, 8)
+            src_ref=src, dst_ref=dst, send_sem=send.at[k], recv_sem=recv.at[k],
+            device_id={"tp": lax.rem(tp + o, TP)}, device_id_type=MESH,
+        )
 
     row, col = iota((n, n), 0), iota((n, n), 1)
     eye = row == col
@@ -277,7 +260,7 @@
 
     unit = keys * lax.rsqrt(by_head(keys * keys) + 1e-06)
     rates = sigmoid(rate_ref[...].astype(F32))
-    extra = jnp.where(first_head, extra_ref[:, :1], extra_ref[:, 1:2])
+    extra = jnp.where(first_head, column_of(extra_ref[:1], eye), column_of(extra_ref[1:2], eye))
     level = 0.6065306597126334
     onward = -level * sigmoid(onward_ref[...].astype(F32)) + extra
     reverse = -level * sigmoid(reverse_ref[...].astype(F32)) + extra
@@ -307,8 +290,30 @@
         value = ref_value.astype(F32)
         return value[:half], value[half : 2 * half], value[n : n + 1], value[n + 8 : n + 9]
 
+    pl.semaphore_wait(barrier, SP - 1 + TP - 1)
     first_copy = pair_copy(element.at[1 - core], partner, 0)
     first_copy.start()
+
+    half_rows = n // 2
+    own_rows = pl.ds(pl.multiple_of(core * half_rows, half_rows), half_rows)
+
+    def block(o):
+        return mixer_w.at[lax.rem(tp + o + TP, TP), own_rows]
+
+    def round_copy(k):
+        o, src = ((1, block(0)), (TP - 1, block(0)), (jnp.where(core == 0, 1, TP - 1), block(jnp.where(core == 0, -1, 1))))[k]
+        return tp_copy(src, src, mixer_send, mixer_recv, k, o)
+
+    def give_copy(o):
+        src = block(o)
+        return pltpu.make_async_remote_copy(
+            src_ref=src, dst_ref=src, send_sem=share_send.at[o], recv_sem=share_recv.at[o],
+            device_id={"sp": sp + sign}, device_id_type=MESH,
+        )
+
+    loads[0].wait()
+    round_copy(0).start()
+    round_copy(1).start()
     first_copy.wait()
     own = element[core].astype(F32)
     own_keep, own_add, own_head, own_tail = own[:half], own[half:n], own[n : n + 1], own[n + 8 : n + 9]
@@ -328,6 +333,50 @@
 
     for k in range(REACH, 0, -1):
         near_copy(k).start()
+
+    lane32, row32 = iota((count, count), 1), iota((count, count), 0)
+    eye32 = lane32 == row32
+    choice = choice_ref[...].astype(F32)
+    lead_line, trail_line = choice[:1], choice[1:2]
+    lead, trail = column_of(lead_line, eye32), column_of(trail_line, eye32)
+    lead_group = jnp.floor(lead * (1.0 / GROUP))
+    group_line = line_of(lead_group, eye32)
+    earlier = lane32 < row32
+
+    def rank(mask):
+        return jnp.sum(jnp.where(earlier & mask, 1.0, 0.0), axis=1, keepdims=True)
+
+    slot = rank(lead_group == group_line)
+    lead_rank = rank((lead == lead_line) | (lead == trail_line))
+    trail_rank = rank((trail == lead_line) | (trail == trail_line))
+    first_weight, second_weight = column_of(route_ref[:1], eye32), column_of(route_ref[1:2], eye32)
+    scale = column_of(group_weight_ref[...], eye32) / (first_weight + second_weight)
+    lane = iota((count, 128), 1).astype(F32)
+    lead_own = lead - GROUP * lead_group + 2 * GROUP * slot
+    trail_own = trail - GROUP * lead_group + 2 * GROUP * slot
+    info = (
+        jnp.where(lane == lead_own, lead_rank + 1.0, 0.0)
+        + jnp.where(lane == trail_own, trail_rank + 1.0, 0.0)
+        + jnp.where(lane == lead_own + GROUP, scale * first_weight, 0.0)
+        + jnp.where(lane == trail_own + GROUP, scale * second_weight, 0.0)
+    )
+    goes = (ahead(iota((SP, count), 0)).astype(F32) == group_line).astype(F32)
+    meta_out[...] = dot(goes, info, precision=HIGHEST).reshape(SP, 1, 128)
+    each(meta_copy, begin)
+    meta_in[SP - 1] = meta_out[SP - 1]
+    stacked = QUARTERS * count
+    group4, slot4 = jnp.concatenate([lead_group] * QUARTERS, 0), jnp.concatenate([slot] * QUARTERS, 0)
+    at, at_row = iota((stacked, size), 1), iota((stacked, size), 0)
+    table = (
+        (group4 == ahead(at >> 4).astype(F32))
+        & (slot4 == (at & 3).astype(F32))
+        & (lax.div(at_row, count) == ((at >> 2) & 3))
+    ).astype(F32)
+    place[...] = table.T.astype(BF16)
+    table = table.astype(BF16)
+    round_copy(0).wait_recv()
+    round_copy(1).wait_recv()
+    round_copy(2).start()
     for k in range(1, REACH + 1):
         near_copy(k).wait_recv()
     keep, add, win_head, tail = parts(near[REACH - 1])
@@ -349,6 +398,9 @@
     far_copy.start()
     for k in range(1, REACH + 1):
         near_copy(k).wait_send()
+    round_copy(2).wait_recv()
+    for o in range(1, TP):
+        give_copy(o).start()
     far_copy.wait()
     far_value = far[...].astype(F32)
     far_tail = jnp.where(exists(REACH), far_value[half : half + 1], -1.0)
@@ -368,110 +420,134 @@
     centred = mixed - by_head(mixed) * (1.0 / HEAD_DIM)
     scaled = centred * lax.rsqrt(by_head(centred * centred) * (1.0 / HEAD_DIM) + 0.00064)
     mix = (scaled * head_scale_ref[...] * sigmoid(out_gate_ref[...].astype(F32))).astype(BF16)
-    loads[0].wait()
-    partial[...] = dot(mix, mixer_w[...]).astype(BF16)
-
-    def share_copy(o):
-        peer = lax.rem(tp + o, TP)
-        src = partial.at[pl.ds(pl.multiple_of(peer * count, count), count)]
-        return tp_copy(src, shares.at[o], tp_send, tp_recv, o, True)
+    for o in range(TP):
+        mix_out[o] = mix[o * count : (o + 1) * count]
+
+    def mix_copy(o):
+        return tp_copy(mix_out.at[lax.rem(tp + o, TP)], mixes.at[tp], mix_send, mix_recv, o, o)
 
     for o in (2, 1, 3):
-        share_copy(o).start()
-    hidden = residual_ref[...].astype(F32)
-    own_share = partial[pl.ds(pl.multiple_of(tp * count, count), count)].astype(F32)
+        mix_copy(o).start()
+    mixes[tp] = mix_out[tp]
+    for o in range(1, TP):
+        give_copy(o).wait_recv()
+    residual = residual_ref[...].astype(F32)
     for o in (1, 3, 2):
-        share_copy(o).wait_recv()
-    shared = own_share + shares[1].astype(F32) + shares[2].astype(F32) + shares[3].astype(F32)
-    hidden = (hidden + shared).astype(BF16).astype(F32)
+        mix_copy(o).wait_recv()
+    wide = jnp.concatenate([mixes[o] for o in range(TP)], axis=1)
+    hidden = residual + dot(wide, mixer_w[...].reshape(TP * n, width))
+    hidden = hidden.astype(BF16).astype(F32)
     normed = (
         hidden * lax.rsqrt(jnp.mean(hidden * hidden, axis=1, keepdims=True) + 1e-06) * expert_scale_ref[...]
     ).astype(BF16)
 
     quarters = jnp.concatenate([normed[:, q * quarter : (q + 1) * quarter] for q in range(QUARTERS)], axis=0)
-    packed[...] = dot(table_rows.T.astype(BF16), quarters).astype(BF16)
-    start_sp(packed, arrived, out_send, out_recv, piece)
-    mine = pl.ds(pl.multiple_of(sp * piece, piece), piece)
-    arrived[mine] = packed[mine]
-
-    wait_sp(meta_out, meta_in, meta_send, meta_recv, 8, "recv")
-    own_meta = pl.ds(pl.multiple_of(sp * 8, 8), 8)
-    meta_in[own_meta] = meta_out[own_meta]
-    size = SP * piece
-    wide_row, wide_col = iota((size, SP * 8), 0), iota((size, SP * 8), 1)
-    widen = ((wide_row >> 4) == (wide_col >> 3)) & ((wide_row & 3) == (wide_col & 7))
-    meta = dot(widen.astype(F32), meta_in[...], precision=HIGHEST)
-    meta_lane = iota((size, 128), 1)
-    taken = SP * CAP
-    t_row, t_col = iota((size, taken), 0), iota((size, taken), 1)
-    same_source = (t_row >> 4) == (t_col >> 1)
-    for o in range(TP):
-        expert = lax.rem(tp + o, TP)
-        code = jnp.sum(jnp.where(meta_lane == expert, meta, 0.0), axis=1, keepdims=True)
-        weight = jnp.sum(jnp.where(meta_lane == expert + GROUP, meta, 0.0), axis=1, keepdims=True)
-        hit = same_source & (code == ((t_col & 1) + 1).astype(F32))
-        for q in range(QUARTERS):
-            here = jnp.where(hit & (((t_row >> 2) & 3) == q), 1.0, 0.0)
-            pick[o, q * taken : (q + 1) * taken] = here.T.astype(BF16)
-            value = here * weight
-            high = value.astype(BF16)
-            at = slice((q * TP + o) * taken, (q * TP + o + 1) * taken)
-            weigh_hi[o, q] = high
-            weigh_lo[o, q] = (value - high.astype(F32)).astype(BF16)
-    wait_sp(packed, arrived, out_send, out_recv, piece, "recv")
-
-    def to_expert(o):
-        return tp_copy(outward.at[o], inbound.at[o], x_send, x_recv, o, True)
-
-    for o in (2, 1, 3, 0):
-        rows = dot(pick[o], arrived[...]).astype(BF16)
-        target = inbound if o == 0 else outward
-        for q in range(QUARTERS):
-            target[o, :, q * quarter : (q + 1) * quarter] = rows[q * taken : (q + 1) * taken]
-        if o:
-            to_expert(o).start()
+    packed[...] = dot(place[...], quarters).astype(BF16)
+    each(out_copy, begin)
+    arrived[size - piece :] = packed[size - piece :]
+
+    each(meta_copy, arrive)
+    told = meta_in[...].reshape(SP, 128)
+    lane = iota((chunk, 128), 1)
+    slot_lane = (iota((chunk, 128), 0) & 3) * (2 * GROUP)
+    cols = QUARTERS * TP * taken
+    row, col = iota((chunk, cols), 0), iota((chunk, cols), 1)
+    col_q, col_o = lax.div(col, TP * taken), lax.rem(lax.div(col, taken), TP)
+    col_k, col_e = lax.rem(lax.div(col, CAP), group_slots), (col & 1) + 1
+    same_place = ((row >> 4) == col_k) & (((row >> 2) & 3) == col_q)
+    source_row, source_col = iota((chunk, SP), 0), iota((chunk, SP), 1)
+    for c in range(CHUNKS):
+        widen = ((source_row >> 4) + c * group_slots == source_col).astype(F32)
+        meta = dot(widen, told, precision=HIGHEST)
+        codes, weights = jnp.zeros((chunk, cols), F32), jnp.zeros((chunk, cols), F32)
+        for o in range(TP):
+            at_code = slot_lane + lax.rem(tp + o, TP)
+            code = jnp.sum(jnp.where(lane == at_code, meta, 0.0), axis=1, keepdims=True)
+            weight = jnp.sum(jnp.where(lane == at_code + GROUP, meta, 0.0), axis=1, keepdims=True)
+            codes, weights = jnp.where(col_o == o, code, codes), jnp.where(col_o == o, weight, weights)
+        hit = same_place & (codes == col_e.astype(F32))
+        pick[c] = jnp.where(hit, 1.0, 0.0).T.astype(BF16)
+        weights = jnp.where(hit, weights, 0.0)
+        high = weights.astype(BF16)
+        weigh_hi[c] = high
+        weigh_lo[c] = (weights - high.astype(F32)).astype(BF16)
+
+    def to_expert(c, o):
+        return tp_copy(outward.at[c, o], inbound.at[c, o], x_send, x_recv, c * TP + o, o)
+
+    def from_expert(c, o):
+        return tp_copy(answers.at[c, o], answered.at[c, o], y_send, y_recv, c * TP + o, TP - o)
+
+    def take(c):
+        each(out_copy, arrive, *bounds(c))
+        rows = dot(pick[c], arrived[c * chunk : (c + 1) * chunk]).astype(BF16)
+        for o in (2, 1, 3, 0):
+            target = outward if o else inbound
+            for q in range(QUARTERS):
+                first = (q * TP + o) * taken
+                target[c, o, :, q * quarter : (q + 1) * quarter] = rows[first : first + taken]
+            if o:
+                to_expert(c, o).start()
+
+    def work(c):
+        for o in (1, 3, 2):
+            to_expert(c, o).wait_recv()
+        rows = inbound[c].reshape(TP * taken, width)
+        gate = dot(rows, gate_w[...])
+        up = dot(rows, up_w[...])
+        active = (gate * sigmoid(gate) * up).astype(BF16)
+        result = dot(active, down_w[...]).astype(BF16)
+        for o in (2, 1, 3, 0):
+            target = answers if o else answered
+            target[c, o] = result[o * taken : (o + 1) * taken]
+            if o:
+                from_expert(c, o).start()
+
+    def give(c):
+        for o in (1, 3, 2):
+            from_expert(c, o).wait_recv()
+        flat = answered[c].reshape(TP * taken, width)
+        flat = jnp.concatenate([flat[:, q * quarter : (q + 1) * quarter] for q in range(QUARTERS)], axis=0)
+        at = slice(c * chunk, (c + 1) * chunk)
+        combined[at] = (dot(weigh_hi[c], flat) + dot(weigh_lo[c], flat)).astype(BF16)
+        each(home_copy, begin, *bounds(c))
+
     for load in loads[1:]:
         load.wait()
-    for o in (1, 3, 2):
-        to_expert(o).wait_recv()
-
-    def back_copy(o):
-        return tp_copy(answers.at[o], answered.at[o], y_send, y_recv, o, False)
-
-    rows = inbound[...].reshape(TP * taken, width)
-    gate = dot(rows, gate_w[...])
-    up = dot(rows, up_w[...])
-    active = (gate * sigmoid(gate) * up).astype(BF16)
-    result = dot(active, down_w[...]).astype(BF16)
-    for o in (2, 1, 3, 0):
-        target = answered if o == 0 else answers
-        target[o] = result[o * taken : (o + 1) * taken]
-        if o:
-            back_copy(o).start()
-    for o in (1, 3, 2):
-        back_copy(o).wait_recv()
-
-    total = jnp.zeros((size, quarter), F32)
-    for o in range(TP):
-        for q in range(QUARTERS):
-            answer = answered[o, :, q * quarter : (q + 1) * quarter]
-            total += dot(weigh_hi[o, q], answer) + dot(weigh_lo[o, q], answer)
-    combined[...] = total.astype(BF16)
-    start_sp(combined, returned, back_send, back_recv, piece)
-    returned[mine] = combined[mine]
-    wait_sp(combined, returned, back_send, back_recv, piece, "recv")
-    final = dot(table_rows.astype(BF16), returned[...])
+    take(0)
+    work(0)
+    take(1)
+    give(0)
+    take(2)
+    take(3)
+    work(1)
+    work(2)
+    give(1)
+    work(3)
+    give(2)
+    give(3)
+    returned[size - piece :] = combined[size - piece :]
+
+    for k in range(3):
+        round_copy(k).wait_send()
+    for o in range(1, TP):
+        give_copy(o).wait_send()
+        mix_copy(o).wait_send()
+        for c in range(CHUNKS):
+            to_expert(c, o).wait_send()
+            from_expert(c, o).wait_send()
+    each(meta_copy, leave)
+    each(out_copy, leave)
+    final = jnp.zeros((stacked, quarter), F32)
+    for c in range(CHUNKS):
+        each(home_copy, arrive, *bounds(c))
+        at = slice(c * chunk, (c + 1) * chunk)
+        final += dot(table[:, at], returned[at])
     for q in range(QUARTERS):
         at = slice(q * quarter, (q + 1) * quarter)
         updated_ref[:, at] = (hidden[:, at] + final[q * count : (q + 1) * count]).astype(BF16)
 
-    for o in range(1, TP):
-        share_copy(o).wait_send()
-        to_expert(o).wait_send()
-        back_copy(o).wait_send()
-    wait_sp(meta_out, meta_in, meta_send, meta_recv, 8, "send")
-    wait_sp(packed, arrived, out_send, out_recv, piece, "send")
-    wait_sp(combined, returned, back_send, back_recv, piece, "send")
+    each(home_copy, leave)
 
 
 def solution(mesh):
@@ -487,7 +563,8 @@
         count, width = residual.shape
         hidden_units = expert_gate_matrix.shape[2]
         piece = QUARTERS * SLOTS
-        size, taken, quarter = SP * piece, SP * CAP, width // QUARTERS
+        size, quarter = SP * piece, width // QUARTERS
+        chunk, taken = size // CHUNKS, SP // CHUNKS * CAP
         vmem, hbm = pl.BlockSpec(memory_space=pltpu.VMEM), pl.BlockSpec(memory_space=pl.ANY)
         dma = pltpu.SemaphoreType.DMA
         return pl.pallas_call(
@@ -503,27 +580,29 @@
                 pltpu.VMEM((n // 2 + 16, n), BF16),
                 pltpu.VMEM((n // 2 + 16, n), BF16),
                 pltpu.VMEM((2, n // 2, n), BF16),
-                pltpu.VMEM((n, width), BF16),
-                pltpu.VMEM((TP, count, width), BF16),
-                pltpu.VMEM((SP * 8, 128), F32),
-                pltpu.VMEM((SP * 8, 128), F32),
+                pltpu.VMEM((TP, count, channels), BF16),
+                pltpu.VMEM((TP, count, channels), BF16),
+                pltpu.VMEM((SP, 1, 128), F32),
+                pltpu.VMEM((SP, 1, 128), F32),
+                pltpu.VMEM((size, QUARTERS * count), BF16),
                 pltpu.VMEM((size, quarter), BF16),
                 pltpu.VMEM((size, quarter), BF16),
-                pltpu.VMEM((TP, QUARTERS * taken, size), BF16),
-                pltpu.VMEM((TP, QUARTERS, size, taken), BF16),
-                pltpu.VMEM((TP, QUARTERS, size, taken), BF16),
-                pltpu.VMEM((TP, taken, width), BF16),
-                pltpu.VMEM((TP, taken, width), BF16),
-                pltpu.VMEM((TP, taken, width), BF16),
-                pltpu.VMEM((TP, taken, width), BF16),
+                pltpu.VMEM((CHUNKS, QUARTERS * TP * taken, chunk), BF16),
+                pltpu.VMEM((CHUNKS, chunk, QUARTERS * TP * taken), BF16),
+                pltpu.VMEM((CHUNKS, chunk, QUARTERS * TP * taken), BF16),
+                pltpu.VMEM((CHUNKS, TP, taken, width), BF16),
+                pltpu.VMEM((CHUNKS, TP, taken, width), BF16),
+                pltpu.VMEM((CHUNKS, TP, taken, width), BF16),
+                pltpu.VMEM((CHUNKS, TP, taken, width), BF16),
                 pltpu.VMEM((size, quarter), BF16),
                 pltpu.VMEM((size, quarter), BF16),
-                pltpu.VMEM((channels, width), BF16),
+                pltpu.VMEM((TP, channels, width), BF16),
                 pltpu.VMEM((width, hidden_units), BF16),
                 pltpu.VMEM((width, hidden_units), BF16),
                 pltpu.VMEM((hidden_units, width), BF16),
-                dma((4,)), dma((4,)), dma((REACH,)), dma((REACH,)), dma((2,)), dma((TP,)), dma((TP,)),
-                dma((SP,)), dma((SP,)), dma((SP,)), dma((SP,)), dma((TP,)), dma((TP,)), dma((TP,)), dma((TP,)),
+                dma((4,)), dma((4,)), dma((REACH,)), dma((REACH,)), dma((2,)), dma((3,)), dma((3,)),
+                dma((TP,)), dma((TP,)), dma((TP,)), dma((TP,)), dma((SP,)), dma((SP,)), dma((SP,)), dma((SP,)),
+                dma((CHUNKS * TP,)), dma((CHUNKS * TP,)), dma((CHUNKS * TP,)), dma((CHUNKS * TP,)),
                 dma((SP,)), dma((SP,)),
             ],
             compiler_params=pltpu.CompilerParams(
@@ -531,9 +610,9 @@
             ),
         )(
             receptance, key_matrix, value_matrix, output_gate_logits, onward_decay_logits, reverse_decay_logits,
-            correction_rate_logits, extra_log_decay, documents.reshape(1, n), head_norm_scale.reshape(1, channels),
-            mixer_output_weight, residual, expert_norm_scale.reshape(1, width), expert_choice_index,
-            group_route_weight.reshape(1, count), expert_route_weight,
+            correction_rate_logits, extra_log_decay.T, documents.reshape(1, n), head_norm_scale.reshape(1, channels),
+            mixer_output_weight, residual, expert_norm_scale.reshape(1, width), expert_choice_index.T,
+            group_route_weight.reshape(1, count), expert_route_weight.T,
             expert_gate_matrix[0], expert_up_matrix[0], expert_down_matrix[0],
         )
 

time: 153 us -> 111 us (0.73)
  Pallas kernels: 147 us -> 108 us
  local copies, waits for them, and re-layouts: 5.69 us -> 1.57 us
    pallas_call x1, Pallas kernels: 147 us -> 108 us  [body(): pl.pallas_call(functools.partial(kernel, (SP, TP)), out_shape=jax.ShapeDt...]
    unnamed x4 -> x1, local copies, waits for them, and re-layouts: 5.69 us -> 1.57 us
where the time goes in v2:
time: 111 us; the launch traced here: 110 us
  Pallas kernels  108 us (97%)
  local copies, waits for them, and re-layouts  1.57 us (1%)
    pallas_call x1, Pallas kernels, body(): pl.pallas_call(functools.partial(kernel, (SP, TP)), out_shape=jax.ShapeDt...  108 us

profile of v2, /device:TPU:33, one launch (start us, length us, event | category | flops | bytes accessed | tf_op | source)
XLA Modules:
  0.0 109.7 jit_solution(4876476569518296502)
XLA Ops:
  0.0 108.1 %shard_map.181 = bf16[32,2048]{1,0:T(8,128)(2,1)} custom-call(bf16[128,128]{1,0:T(8,128)(2,1)} %refs_0_.1, bf16[128,128]{1,0:T(8,128)(2,1)} %refs_1_.1, bf16[128,128]{1,0:T(8,128)(2,1)} %refs_2_.1, bf16[128,128]{1,0:T(8,128)(2,1)} %refs_3_.1, bf16[128,128]{1,0:T(8,128)(2,1)} %refs_4_.1, bf16[128,128]{1,0:T(8,128)(2,1)} %refs_5_.1, bf16[128,128]{1,0:T(8,128)(2,1)} %refs_6_.1, ...), custom_call_target="tpu_custom_call" | custom-call | tf_op jit(solution)/shard_map/pallas_call | solution.py:570
  108.1 1.6 %copy.21 = bf16[32,2048]{1,0:T(8,128)(2,1)} copy(bf16[32,2048]{1,0:T(8,128)(2,1)} %shard_map.181) | data formatting | bytes 262144

commit v3 on v2

--- a/solution.py
+++ b/solution.py
@@ -97,7 +97,7 @@
     left = jnp.concatenate([probe, lifted], axis=0)
     right = jnp.concatenate([fix_keys, add_keys], axis=0).astype(BF16)
     values_low = values.astype(BF16)
-    removed, added, reads = [], [], []
+    added, reads, inverses, sources = [], [], [], []
     for head in range(2):
         mine = first_head if head == 0 else jnp.logical_not(first_head)
         grams = low(jnp.where(mine, left, 0.0), right, LANES)
@@ -107,8 +107,10 @@
         read_add = jnp.where(inclusive, grams[n:, n:], 0.0)
         mixed = low(jnp.concatenate([add_mix, read_add], axis=0), values_low)
         added.append(mixed[n:])
-        source = -jnp.concatenate([mixed[:n], probe_open], axis=1)
-        removed.append(low(inverse(system, row, col), source))
+        sources.append(-jnp.concatenate([mixed[:n], probe_open], axis=1))
+        inverses.append(inverse(system, row, col))
+    yield None
+    removed = [low(inverses[head], sources[head]) for head in range(2)]
     both = jnp.concatenate([first_head, first_head], axis=1)
     took = jnp.where(both, removed[0], removed[1])
     heads = [low(reads[head], took) for head in range(2)]
@@ -131,7 +133,7 @@
         ],
         axis=0,
     ).astype(BF16)
-    return outputs, response, element
+    yield outputs, response, element
 
 
 def spread(block, same_head):
@@ -148,13 +150,13 @@
         docs_ref, head_scale_ref, mixer_hbm, residual_ref, expert_scale_ref, choice_ref, group_weight_ref,
         route_ref, gate_hbm, up_hbm, down_hbm,
         updated_ref,
-        element, partner, chip, near, window, far, entering,
-        mix_out, mixes, meta_out, meta_in, place, packed, arrived, pick, weigh_hi, weigh_lo,
-        outward, inbound, answers, answered, combined, returned,
+        element, partner, chip, came, far, entering,
+        mix_out, mixes, meta_out, meta_in, place, packed, arrived, packed_mix, arrived_mix, pick, weigh_hi, weigh_lo,
+        outward, inbound, outward_mix, inbound_mix, answers, answered, combined, returned,
         mixer_w, gate_w, up_w, down_w,
-        w_sem, pair_sem, near_send, near_recv, far_sem, mixer_send, mixer_recv, share_send, share_recv,
-        mix_send, mix_recv, meta_send, meta_recv, out_send, out_recv, x_send, x_recv, y_send, y_recv,
-        back_send, back_recv,
+        w_sem, pair_sem, scan_send, scan_recv, mixer_send, mixer_recv, share_send, share_recv,
+        mix_send, mix_recv, meta_send, meta_recv, out_send, out_recv, late_send, late_recv, x_send, x_recv,
+        m_send, m_recv, y_send, y_recv,        back_send, back_recv,
     ) = refs
     SP, TP = sizes
     chips = SP // 2
@@ -190,6 +192,8 @@
 
     def turn(k):
         half = (k + 1) >> 1
+        if isinstance(k, int):
+            return SP // 2 + (-half if k & 1 else half)
         return SP // 2 + jnp.where((k & 1) == 1, -half, half)
 
     def ahead(k):
@@ -215,18 +219,26 @@
     def out_copy(k):
         return sp_copy(rows_at(packed, k), rows_at(arrived, k), out_send, out_recv, k)
 
+    def late_copy(k):
+        return sp_copy(rows_at(packed_mix, k), rows_at(arrived_mix, k), late_send, late_recv, k)
+
     def home_copy(k):
         return sp_copy(rows_at(combined, k), rows_at(returned, k), back_send, back_recv, k, True)
 
+    def begin(copy):
+        copy.start()
+
     def each(make, act, first=0, last=SP - 1):
+        if act is begin:
+            for k in range(first, last):
+                act(make(k))
+            return
+
         def one(k, carry):
             act(make(k))
             return carry
 
         lax.fori_loop(first, last, one, 0)
-
-    def begin(copy):
-        copy.start()
 
     def leave(copy):
         copy.wait_send()
@@ -242,97 +254,6 @@
             src_ref=src, dst_ref=dst, send_sem=send.at[k], recv_sem=recv.at[k],
             device_id={"tp": lax.rem(tp + o, TP)}, device_id_type=MESH,
         )
-
-    row, col = iota((n, n), 0), iota((n, n), 1)
-    eye = row == col
-    same_head = (row < HEAD_DIM) == (col < HEAD_DIM)
-    first_head = iota((1, n), 1) < HEAD_DIM
-    doc_row = docs_ref[...].astype(F32)
-    doc_col = column_of(doc_row, eye)
-    reader = receptance_ref[...].astype(F32)
-    keys = key_ref[...].astype(F32)
-    values = value_ref[...].astype(F32)
-
-    def by_head(x):
-        one = jnp.sum(jnp.where(first_head, x, 0.0), axis=1, keepdims=True)
-        two = jnp.sum(jnp.where(first_head, 0.0, x), axis=1, keepdims=True)
-        return jnp.where(first_head, one, two)
-
-    unit = keys * lax.rsqrt(by_head(keys * keys) + 1e-06)
-    rates = sigmoid(rate_ref[...].astype(F32))
-    extra = jnp.where(first_head, column_of(extra_ref[:1], eye), column_of(extra_ref[1:2], eye))
-    level = 0.6065306597126334
-    onward = -level * sigmoid(onward_ref[...].astype(F32)) + extra
-    reverse = -level * sigmoid(reverse_ref[...].astype(F32)) + extra
-    out_f, resp_f, element_f = direction(reader, keys, values, unit, rates, onward, doc_col, doc_row, False)
-    out_b, resp_b, element_b = direction(reader, keys, values, unit, rates, reverse, doc_col, doc_row, True)
-    element[0] = element_f
-    element[1] = element_b
-
-    sign = 1 - 2 * core
-
-    def pair_copy(src, dst, k):
-        return pltpu.make_async_remote_copy(
-            src_ref=src, dst_ref=dst, send_sem=pair_sem.at[2 * k], recv_sem=pair_sem.at[2 * k + 1],
-            device_id={"sp": sp + sign}, device_id_type=MESH,
-        )
-
-    def chip_peer(distance):
-        return lax.rem(z + sign * distance + chips, chips) * 2 + core
-
-    def exists(distance):
-        origin = z - sign * distance
-        return (origin >= 0) & (origin < chips)
-
-    half = n // 2
-
-    def parts(ref_value):
-        value = ref_value.astype(F32)
-        return value[:half], value[half : 2 * half], value[n : n + 1], value[n + 8 : n + 9]
-
-    pl.semaphore_wait(barrier, SP - 1 + TP - 1)
-    first_copy = pair_copy(element.at[1 - core], partner, 0)
-    first_copy.start()
-
-    half_rows = n // 2
-    own_rows = pl.ds(pl.multiple_of(core * half_rows, half_rows), half_rows)
-
-    def block(o):
-        return mixer_w.at[lax.rem(tp + o + TP, TP), own_rows]
-
-    def round_copy(k):
-        o, src = ((1, block(0)), (TP - 1, block(0)), (jnp.where(core == 0, 1, TP - 1), block(jnp.where(core == 0, -1, 1))))[k]
-        return tp_copy(src, src, mixer_send, mixer_recv, k, o)
-
-    def give_copy(o):
-        src = block(o)
-        return pltpu.make_async_remote_copy(
-            src_ref=src, dst_ref=src, send_sem=share_send.at[o], recv_sem=share_recv.at[o],
-            device_id={"sp": sp + sign}, device_id_type=MESH,
-        )
-
-    loads[0].wait()
-    round_copy(0).start()
-    round_copy(1).start()
-    first_copy.wait()
-    own = element[core].astype(F32)
-    own_keep, own_add, own_head, own_tail = own[:half], own[half:n], own[n : n + 1], own[n + 8 : n + 9]
-    par_keep, par_add, par_head, par_tail = parts(partner[...])
-    joined = link(own_tail, par_head)
-    both = joined * low(own[:n], spread(par_keep, same_head))
-    chip[...] = jnp.concatenate(
-        [both[:half], both[half:] + par_add, jnp.broadcast_to(own_head, (8, n)), jnp.broadcast_to(par_tail, (8, n))],
-        axis=0,
-    ).astype(BF16)
-
-    def near_copy(k):
-        return pltpu.make_async_remote_copy(
-            src_ref=chip, dst_ref=near.at[k - 1], send_sem=near_send.at[k - 1], recv_sem=near_recv.at[k - 1],
-            device_id={"sp": chip_peer(k)}, device_id_type=MESH,
-        )
-
-    for k in range(REACH, 0, -1):
-        near_copy(k).start()
 
     lane32, row32 = iota((count, count), 1), iota((count, count), 0)
     eye32 = lane32 == row32
@@ -362,8 +283,6 @@
     )
     goes = (ahead(iota((SP, count), 0)).astype(F32) == group_line).astype(F32)
     meta_out[...] = dot(goes, info, precision=HIGHEST).reshape(SP, 1, 128)
-    each(meta_copy, begin)
-    meta_in[SP - 1] = meta_out[SP - 1]
     stacked = QUARTERS * count
     group4, slot4 = jnp.concatenate([lead_group] * QUARTERS, 0), jnp.concatenate([slot] * QUARTERS, 0)
     at, at_row = iota((stacked, size), 1), iota((stacked, size), 0)
@@ -374,77 +293,145 @@
     ).astype(F32)
     place[...] = table.T.astype(BF16)
     table = table.astype(BF16)
+
+    def by_quarter(rows):
+        part = rows.shape[1] // QUARTERS
+        return jnp.concatenate([rows[:, q * part : (q + 1) * part] for q in range(QUARTERS)], axis=0)
+
+    packed[...] = dot(place[...], by_quarter(residual_ref[...])).astype(BF16)
+
+    row, col = iota((n, n), 0), iota((n, n), 1)
+    eye = row == col
+    same_head = (row < HEAD_DIM) == (col < HEAD_DIM)
+    first_head = iota((1, n), 1) < HEAD_DIM
+    doc_row = docs_ref[...].astype(F32)
+    doc_col = column_of(doc_row, eye)
+    reader = receptance_ref[...].astype(F32)
+    keys = key_ref[...].astype(F32)
+    values = value_ref[...].astype(F32)
+
+    def by_head(x):
+        one = jnp.sum(jnp.where(first_head, x, 0.0), axis=1, keepdims=True)
+        two = jnp.sum(jnp.where(first_head, 0.0, x), axis=1, keepdims=True)
+        return jnp.where(first_head, one, two)
+
+    unit = keys * lax.rsqrt(by_head(keys * keys) + 1e-06)
+    rates = sigmoid(rate_ref[...].astype(F32))
+    extra = jnp.where(first_head, column_of(extra_ref[:1], eye), column_of(extra_ref[1:2], eye))
+    level = 0.6065306597126334
+    onward = -level * sigmoid(onward_ref[...].astype(F32)) + extra
+    reverse = -level * sigmoid(reverse_ref[...].astype(F32)) + extra
+    forward = direction(reader, keys, values, unit, rates, onward, doc_col, doc_row, False)
+    backward = direction(reader, keys, values, unit, rates, reverse, doc_col, doc_row, True)
+    next(forward)
+    next(backward)
+
+    pl.semaphore_wait(barrier, SP - 1 + TP - 1)
+
+    out_f, resp_f, element_f = next(forward)
+    out_b, resp_b, element_b = next(backward)
+    element[0] = element_f
+    element[1] = element_b
+
+    sign = 1 - 2 * core
+
+    def pair_copy(src, dst, k):
+        return pltpu.make_async_remote_copy(
+            src_ref=src, dst_ref=dst, send_sem=pair_sem.at[2 * k], recv_sem=pair_sem.at[2 * k + 1],
+            device_id={"sp": sp + sign}, device_id_type=MESH,
+        )
+
+    def chip_peer(distance):
+        return lax.rem(z + sign * distance + chips, chips) * 2 + core
+
+    def exists(distance):
+        origin = z - sign * distance
+        return (origin >= 0) & (origin < chips)
+
+    half = n // 2
+
+    def parts(ref_value):
+        value = ref_value.astype(F32)
+        return value[:half], value[half : 2 * half], value[n : n + 1], value[n + 8 : n + 9]
+
+    first_copy = pair_copy(element.at[1 - core], partner, 0)
+    first_copy.start()
+
+    half_rows = n // 2
+    own_rows = pl.ds(pl.multiple_of(core * half_rows, half_rows), half_rows)
+
+    def block(o):
+        return mixer_w.at[lax.rem(tp + o + TP, TP), own_rows]
+
+    def round_copy(k):
+        o, src = ((1, block(0)), (TP - 1, block(0)), (jnp.where(core == 0, 1, TP - 1), block(jnp.where(core == 0, -1, 1))))[k]
+        return tp_copy(src, src, mixer_send, mixer_recv, k, o)
+
+    def give_copy(o):
+        src = block(o)
+        return pltpu.make_async_remote_copy(
+            src_ref=src, dst_ref=src, send_sem=share_send.at[o], recv_sem=share_recv.at[o],
+            device_id={"sp": sp + sign}, device_id_type=MESH,
+        )
+
+    loads[0].wait()
+    round_copy(0).start()
+    round_copy(1).start()
+    each(meta_copy, begin)
+    meta_in[SP - 1] = meta_out[SP - 1]
+    each(out_copy, begin, *bounds(3))
+    arrived[size - piece :] = packed[size - piece :]
+    first_copy.wait()
+    own = element[core].astype(F32)
+    own_keep, own_add, own_head, own_tail = own[:half], own[half:n], own[n : n + 1], own[n + 8 : n + 9]
+    par_keep, par_add, par_head, par_tail = parts(partner[...])
+    joined = link(own_tail, par_head)
+    both = joined * low(own[:n], spread(par_keep, same_head))
+    def keep_element(at, both, head, tail):
+        chip[at] = jnp.concatenate(
+            [both, jnp.broadcast_to(head, (8, n)), jnp.broadcast_to(tail, (8, n))], axis=0
+        ).astype(BF16)
+
+    zeros = jnp.zeros((half, n), F32)
+    window = both + jnp.concatenate([zeros, par_add], axis=0)
+    head, tail = own_head, par_tail
+
+    def scan_copy(k):
+        src, dst, distance = (
+            (chip.at[0], came.at[0], 1),
+            (chip.at[1], came.at[1], 2),
+            (chip.at[2], came.at[2], 1),
+            (far.at[0], far.at[1], REACH + 1),
+        )[k]
+        return pltpu.make_async_remote_copy(
+            src_ref=src, dst_ref=dst, send_sem=scan_send.at[k], recv_sem=scan_recv.at[k],
+            device_id={"sp": chip_peer(distance)}, device_id_type=MESH,
+        )
+
+    def doubled(k, distance, window, head):
+        past_keep, past_add, past_head, past_tail = parts(came[k])
+        past_tail = jnp.where(exists(distance), past_tail, -1.0)
+        joined = link(past_tail, head) * low(
+            jnp.concatenate([past_keep, past_add], axis=0), spread(window[:half], same_head)
+        )
+        return joined + jnp.concatenate([zeros, window[half:]], axis=0), past_head
+
+    keep_element(0, window, head, tail)
+    scan_copy(0).start()
+    scan_copy(0).wait_recv()
+    window, head = doubled(0, 1, window, head)
+    keep_element(1, window, head, tail)
+    scan_copy(1).start()
     round_copy(0).wait_recv()
     round_copy(1).wait_recv()
     round_copy(2).start()
-    for k in range(1, REACH + 1):
-        near_copy(k).wait_recv()
-    keep, add, win_head, tail = parts(near[REACH - 1])
-    tail = jnp.where(exists(REACH), tail, -1.0)
-    for k in range(REACH - 1, 0, -1):
-        next_keep, next_add, next_head, next_tail = parts(near[k - 1])
-        step = link(tail, next_head) * low(
-            jnp.concatenate([keep, add], axis=0), spread(next_keep, same_head)
-        )
-        keep, add = step[:half], step[half:] + next_add
-        tail = jnp.where(exists(k), next_tail, -1.0)
-    window[...] = jnp.concatenate(
-        [add, jnp.broadcast_to(tail, (16, n))], axis=0
-    ).astype(BF16)
-    far_copy = pltpu.make_async_remote_copy(
-        src_ref=window, dst_ref=far, send_sem=far_sem.at[0], recv_sem=far_sem.at[1],
-        device_id={"sp": chip_peer(REACH)}, device_id_type=MESH,
-    )
-    far_copy.start()
-    for k in range(1, REACH + 1):
-        near_copy(k).wait_send()
-    round_copy(2).wait_recv()
-    for o in range(1, TP):
-        give_copy(o).start()
-    far_copy.wait()
-    far_value = far[...].astype(F32)
-    far_tail = jnp.where(exists(REACH), far_value[half : half + 1], -1.0)
-    add = add + link(far_tail, win_head) * low(far_value[:half], spread(keep, same_head))
-    state = link(tail, own_head) * add
-    passed = (low(state, spread(own_keep, same_head)) + own_add) * joined
-    entering[0] = passed.astype(BF16)
-    last_copy = pair_copy(entering.at[0], entering.at[1], 1)
-    last_copy.start()
-    last_copy.wait()
-    other = entering[1].astype(F32)
-    state_f = jnp.where(core == 0, state, other)
-    state_b = jnp.where(core == 0, other, state)
-    entry = jnp.concatenate([spread(state_f, same_head), spread(state_b, same_head)], axis=1)
-    mixed = out_f + out_b + low(jnp.concatenate([resp_f, resp_b], axis=1), entry, LANES)
-
-    centred = mixed - by_head(mixed) * (1.0 / HEAD_DIM)
-    scaled = centred * lax.rsqrt(by_head(centred * centred) * (1.0 / HEAD_DIM) + 0.00064)
-    mix = (scaled * head_scale_ref[...] * sigmoid(out_gate_ref[...].astype(F32))).astype(BF16)
-    for o in range(TP):
-        mix_out[o] = mix[o * count : (o + 1) * count]
-
-    def mix_copy(o):
-        return tp_copy(mix_out.at[lax.rem(tp + o, TP)], mixes.at[tp], mix_send, mix_recv, o, o)
-
-    for o in (2, 1, 3):
-        mix_copy(o).start()
-    mixes[tp] = mix_out[tp]
-    for o in range(1, TP):
-        give_copy(o).wait_recv()
-    residual = residual_ref[...].astype(F32)
-    for o in (1, 3, 2):
-        mix_copy(o).wait_recv()
-    wide = jnp.concatenate([mixes[o] for o in range(TP)], axis=1)
-    hidden = residual + dot(wide, mixer_w[...].reshape(TP * n, width))
-    hidden = hidden.astype(BF16).astype(F32)
-    normed = (
-        hidden * lax.rsqrt(jnp.mean(hidden * hidden, axis=1, keepdims=True) + 1e-06) * expert_scale_ref[...]
-    ).astype(BF16)
-
-    quarters = jnp.concatenate([normed[:, q * quarter : (q + 1) * quarter] for q in range(QUARTERS)], axis=0)
-    packed[...] = dot(place[...], quarters).astype(BF16)
-    each(out_copy, begin)
-    arrived[size - piece :] = packed[size - piece :]
+    scan_copy(1).wait_recv()
+    window, head = doubled(1, 2, window, head)
+    far[0] = jnp.concatenate([window[half:], jnp.broadcast_to(tail, (16, n))], axis=0).astype(BF16)
+    scan_copy(3).start()
+    keep_element(2, window, head, tail)
+    scan_copy(2).start()
+    each(out_copy, begin, *bounds(2))
 
     each(meta_copy, arrive)
     told = meta_in[...].reshape(SP, 128)
@@ -472,27 +459,88 @@
         weigh_hi[c] = high
         weigh_lo[c] = (weights - high.astype(F32)).astype(BF16)
 
+    round_copy(2).wait_recv()
+    for o in range(1, TP):
+        give_copy(o).start()
+    scan_copy(2).wait_recv()
+    keep, add, past_head, past_tail = parts(came[2])
+    keep = spread(keep, same_head)
+    scan_copy(3).wait_recv()
+    far_value = far[1].astype(F32)
+    far_tail = jnp.where(exists(REACH + 1), far_value[half : half + 1], -1.0)
+    add = add + link(far_tail, past_head) * low(far_value[:half], keep)
+    tail = jnp.where(exists(1), past_tail, -1.0)
+    state = link(tail, own_head) * add
+    passed = (low(state, spread(own_keep, same_head)) + own_add) * joined
+    entering[0] = passed.astype(BF16)
+    last_copy = pair_copy(entering.at[0], entering.at[1], 1)
+    last_copy.start()
+    each(out_copy, begin, *bounds(0))
+    last_copy.wait()
+    other = entering[1].astype(F32)
+    state_f = jnp.where(core == 0, state, other)
+    state_b = jnp.where(core == 0, other, state)
+    entry = jnp.concatenate([spread(state_f, same_head), spread(state_b, same_head)], axis=1)
+    mixed = out_f + out_b + low(jnp.concatenate([resp_f, resp_b], axis=1), entry, LANES)
+
+    centred = mixed - by_head(mixed) * (1.0 / HEAD_DIM)
+    scaled = centred * lax.rsqrt(by_head(centred * centred) * (1.0 / HEAD_DIM) + 0.00064)
+    mix = (scaled * head_scale_ref[...] * sigmoid(out_gate_ref[...].astype(F32))).astype(BF16)
+    for o in range(TP):
+        mix_out[o] = mix[o * count : (o + 1) * count]
+
+    def mix_copy(o):
+        return tp_copy(mix_out.at[lax.rem(tp + o, TP)], mixes.at[tp], mix_send, mix_recv, o, o)
+
+    for o in (2, 1, 3):
+        mix_copy(o).start()
+    mixes[tp] = mix_out[tp]
+    for o in (1, 3, 2):
+        mix_copy(o).wait_recv()
+    packed_mix[...] = dot(place[...], mixes[...].reshape(TP * count, n)).astype(BF16)
+    each(late_copy, begin, *bounds(2))
+    each(late_copy, begin, *bounds(0))
+    each(late_copy, begin, *bounds(1))
+    each(late_copy, begin, *bounds(3))
+    each(out_copy, begin, *bounds(1))
+    arrived_mix[size - piece :] = packed_mix[size - piece :]
+
     def to_expert(c, o):
         return tp_copy(outward.at[c, o], inbound.at[c, o], x_send, x_recv, c * TP + o, o)
 
+    def to_expert_mix(c, o):
+        return tp_copy(outward_mix.at[c, o], inbound_mix.at[c, o], m_send, m_recv, c * TP + o, o)
+
     def from_expert(c, o):
         return tp_copy(answers.at[c, o], answered.at[c, o], y_send, y_recv, c * TP + o, TP - o)
 
-    def take(c):
-        each(out_copy, arrive, *bounds(c))
-        rows = dot(pick[c], arrived[c * chunk : (c + 1) * chunk]).astype(BF16)
+    def take(c, copy, source, theirs, ours, send):
+        each(copy, arrive, *bounds(c))
+        rows = dot(pick[c], source[c * chunk : (c + 1) * chunk]).astype(BF16)
+        part = rows.shape[1]
         for o in (2, 1, 3, 0):
-            target = outward if o else inbound
+            target = theirs if o else ours
             for q in range(QUARTERS):
                 first = (q * TP + o) * taken
-                target[c, o, :, q * quarter : (q + 1) * quarter] = rows[first : first + taken]
+                target[c, o, :, q * part : (q + 1) * part] = rows[first : first + taken]
             if o:
-                to_expert(c, o).start()
+                send(c, o).start()
+
+    def norm(rows):
+        rows = rows * lax.rsqrt(jnp.mean(rows * rows, axis=1, keepdims=True) + 1e-06)
+        return (rows * expert_scale_ref[...]).astype(BF16)
+
+    def project(rows, channels):
+        rows = rows.astype(F32) + dot(channels, mixer_w[...].reshape(TP * n, width))
+        return rows.astype(BF16).astype(F32)
 
     def work(c):
         for o in (1, 3, 2):
             to_expert(c, o).wait_recv()
+        for o in (1, 3, 2):
+            to_expert_mix(c, o).wait_recv()
         rows = inbound[c].reshape(TP * taken, width)
+        rows = norm(project(rows, inbound_mix[c].reshape(TP * taken, TP * n)))
         gate = dot(rows, gate_w[...])
         up = dot(rows, up_w[...])
         active = (gate * sigmoid(gate) * up).astype(BF16)
@@ -507,37 +555,54 @@
         for o in (1, 3, 2):
             from_expert(c, o).wait_recv()
         flat = answered[c].reshape(TP * taken, width)
-        flat = jnp.concatenate([flat[:, q * quarter : (q + 1) * quarter] for q in range(QUARTERS)], axis=0)
+        flat = by_quarter(flat)
         at = slice(c * chunk, (c + 1) * chunk)
         combined[at] = (dot(weigh_hi[c], flat) + dot(weigh_lo[c], flat)).astype(BF16)
         each(home_copy, begin, *bounds(c))
 
     for load in loads[1:]:
         load.wait()
-    take(0)
+    def take_early(c):
+        take(c, out_copy, arrived, outward, inbound, to_expert)
+
+    def take_late(c):
+        take(c, late_copy, arrived_mix, outward_mix, inbound_mix, to_expert_mix)
+
+    take_early(3)
+    take_early(2)
+    take_early(0)
+    for o in range(1, TP):
+        give_copy(o).wait_recv()
+    hidden = project(residual_ref[...], jnp.concatenate([mixes[o] for o in range(TP)], axis=1))
+    take_late(2)
+    take_late(0)
+    take_late(3)
+    take_late(1)
+    work(2)
+    take_early(1)
     work(0)
-    take(1)
-    give(0)
-    take(2)
-    take(3)
-    work(1)
-    work(2)
-    give(1)
     work(3)
     give(2)
+    give(0)
+    work(1)
     give(3)
+    give(1)
     returned[size - piece :] = combined[size - piece :]
 
     for k in range(3):
         round_copy(k).wait_send()
+    for k in range(4):
+        scan_copy(k).wait_send()
     for o in range(1, TP):
         give_copy(o).wait_send()
         mix_copy(o).wait_send()
         for c in range(CHUNKS):
             to_expert(c, o).wait_send()
+            to_expert_mix(c, o).wait_send()
             from_expert(c, o).wait_send()
     each(meta_copy, leave)
     each(out_copy, leave)
+    each(late_copy, leave)
     final = jnp.zeros((stacked, quarter), F32)
     for c in range(CHUNKS):
         each(home_copy, arrive, *bounds(c))
@@ -575,10 +640,9 @@
             scratch_shapes=[
                 pltpu.VMEM((2, n + 16, n), BF16),
                 pltpu.VMEM((n + 16, n), BF16),
-                pltpu.VMEM((n + 16, n), BF16),
-                pltpu.VMEM((REACH, n + 16, n), BF16),
-                pltpu.VMEM((n // 2 + 16, n), BF16),
-                pltpu.VMEM((n // 2 + 16, n), BF16),
+                pltpu.VMEM((4, n + 16, n), BF16),
+                pltpu.VMEM((3, n + 16, n), BF16),
+                pltpu.VMEM((2, n // 2 + 16, n), BF16),
                 pltpu.VMEM((2, n // 2, n), BF16),
                 pltpu.VMEM((TP, count, channels), BF16),
                 pltpu.VMEM((TP, count, channels), BF16),
@@ -587,11 +651,15 @@
                 pltpu.VMEM((size, QUARTERS * count), BF16),
                 pltpu.VMEM((size, quarter), BF16),
                 pltpu.VMEM((size, quarter), BF16),
+                pltpu.VMEM((size, channels), BF16),
+                pltpu.VMEM((size, channels), BF16),
                 pltpu.VMEM((CHUNKS, QUARTERS * TP * taken, chunk), BF16),
                 pltpu.VMEM((CHUNKS, chunk, QUARTERS * TP * taken), BF16),
                 pltpu.VMEM((CHUNKS, chunk, QUARTERS * TP * taken), BF16),
                 pltpu.VMEM((CHUNKS, TP, taken, width), BF16),
                 pltpu.VMEM((CHUNKS, TP, taken, width), BF16),
+                pltpu.VMEM((CHUNKS, TP, taken, TP * channels), BF16),
+                pltpu.VMEM((CHUNKS, TP, taken, TP * channels), BF16),
                 pltpu.VMEM((CHUNKS, TP, taken, width), BF16),
                 pltpu.VMEM((CHUNKS, TP, taken, width), BF16),
                 pltpu.VMEM((size, quarter), BF16),
@@ -600,9 +668,10 @@
                 pltpu.VMEM((width, hidden_units), BF16),
                 pltpu.VMEM((width, hidden_units), BF16),
                 pltpu.VMEM((hidden_units, width), BF16),
-                dma((4,)), dma((4,)), dma((REACH,)), dma((REACH,)), dma((2,)), dma((3,)), dma((3,)),
+                dma((4,)), dma((4,)), dma((4,)), dma((4,)), dma((3,)), dma((3,)),
                 dma((TP,)), dma((TP,)), dma((TP,)), dma((TP,)), dma((SP,)), dma((SP,)), dma((SP,)), dma((SP,)),
-                dma((CHUNKS * TP,)), dma((CHUNKS * TP,)), dma((CHUNKS * TP,)), dma((CHUNKS * TP,)),
+                dma((SP,)), dma((SP,)), dma((CHUNKS * TP,)), dma((CHUNKS * TP,)), dma((CHUNKS * TP,)),
+                dma((CHUNKS * TP,)), dma((CHUNKS * TP,)), dma((CHUNKS * TP,)),
                 dma((SP,)), dma((SP,)),
             ],
             compiler_params=pltpu.CompilerParams(

time: 111 us -> 110 us (level)
  no operation moved by 1% of the time
where the time goes in v3:
time: 110 us
  Pallas kernels  108 us (98%)
  local copies, waits for them, and re-layouts  1.57 us (1%)
    pallas_call x1, Pallas kernels, body(): pl.pallas_call(functools.partial(kernel, (SP, TP)), out_shape=jax.ShapeDt...  108 us

profile of v3, /device:TPU:33, one launch (start us, length us, event | category | flops | bytes accessed | tf_op | source)
XLA Modules:
  0.0 109.6 jit_solution(15589978141589935064)
XLA Ops:
  0.0 108.0 %shard_map.181 = bf16[32,2048]{1,0:T(8,128)(2,1)} custom-call(bf16[128,128]{1,0:T(8,128)(2,1)} %refs_0_.1, bf16[128,128]{1,0:T(8,128)(2,1)} %refs_1_.1, bf16[128,128]{1,0:T(8,128)(2,1)} %refs_2_.1, bf16[128,128]{1,0:T(8,128)(2,1)} %refs_3_.1, bf16[128,128]{1,0:T(8,128)(2,1)} %refs_4_.1, bf16[128,128]{1,0:T(8,128)(2,1)} %refs_5_.1, bf16[128,128]{1,0:T(8,128)(2,1)} %refs_6_.1, ...), custom_call_target="tpu_custom_call" | custom-call | tf_op jit(solution)/shard_map/pallas_call | solution.py:635
  108.0 1.6 %copy.21 = bf16[32,2048]{1,0:T(8,128)(2,1)} copy(bf16[32,2048]{1,0:T(8,128)(2,1)} %shard_map.181) | data formatting | bytes 262144

commit v4 on v2

--- a/solution.py
+++ b/solution.py
@@ -148,11 +148,11 @@
         docs_ref, head_scale_ref, mixer_hbm, residual_ref, expert_scale_ref, choice_ref, group_weight_ref,
         route_ref, gate_hbm, up_hbm, down_hbm,
         updated_ref,
-        element, partner, chip, near, window, far, entering,
+        element, partner, chip, came, far, entering,
         mix_out, mixes, meta_out, meta_in, place, packed, arrived, pick, weigh_hi, weigh_lo,
         outward, inbound, answers, answered, combined, returned,
         mixer_w, gate_w, up_w, down_w,
-        w_sem, pair_sem, near_send, near_recv, far_sem, mixer_send, mixer_recv, share_send, share_recv,
+        w_sem, pair_sem, scan_send, scan_recv, mixer_send, mixer_recv, share_send, share_recv,
         mix_send, mix_recv, meta_send, meta_recv, out_send, out_recv, x_send, x_recv, y_send, y_recv,
         back_send, back_recv,
     ) = refs
@@ -190,6 +190,8 @@
 
     def turn(k):
         half = (k + 1) >> 1
+        if isinstance(k, int):
+            return SP // 2 + (-half if k & 1 else half)
         return SP // 2 + jnp.where((k & 1) == 1, -half, half)
 
     def ahead(k):
@@ -218,15 +220,20 @@
     def home_copy(k):
         return sp_copy(rows_at(combined, k), rows_at(returned, k), back_send, back_recv, k, True)
 
+    def begin(copy):
+        copy.start()
+
     def each(make, act, first=0, last=SP - 1):
+        if act is begin:
+            for k in range(first, last):
+                act(make(k))
+            return
+
         def one(k, carry):
             act(make(k))
             return carry
 
         lax.fori_loop(first, last, one, 0)
-
-    def begin(copy):
-        copy.start()
 
     def leave(copy):
         copy.wait_send()
@@ -320,19 +327,37 @@
     par_keep, par_add, par_head, par_tail = parts(partner[...])
     joined = link(own_tail, par_head)
     both = joined * low(own[:n], spread(par_keep, same_head))
-    chip[...] = jnp.concatenate(
-        [both[:half], both[half:] + par_add, jnp.broadcast_to(own_head, (8, n)), jnp.broadcast_to(par_tail, (8, n))],
-        axis=0,
-    ).astype(BF16)
-
-    def near_copy(k):
+    def keep_element(at, both, head, tail):
+        chip[at] = jnp.concatenate(
+            [both, jnp.broadcast_to(head, (8, n)), jnp.broadcast_to(tail, (8, n))], axis=0
+        ).astype(BF16)
+
+    zeros = jnp.zeros((half, n), F32)
+    window = both + jnp.concatenate([zeros, par_add], axis=0)
+    head, tail = own_head, par_tail
+
+    def scan_copy(k):
+        src, dst, distance = (
+            (chip.at[0], came.at[0], 1),
+            (chip.at[1], came.at[1], 2),
+            (chip.at[2], came.at[2], 1),
+            (far.at[0], far.at[1], REACH + 1),
+        )[k]
         return pltpu.make_async_remote_copy(
-            src_ref=chip, dst_ref=near.at[k - 1], send_sem=near_send.at[k - 1], recv_sem=near_recv.at[k - 1],
-            device_id={"sp": chip_peer(k)}, device_id_type=MESH,
-        )
-
-    for k in range(REACH, 0, -1):
-        near_copy(k).start()
+            src_ref=src, dst_ref=dst, send_sem=scan_send.at[k], recv_sem=scan_recv.at[k],
+            device_id={"sp": chip_peer(distance)}, device_id_type=MESH,
+        )
+
+    def doubled(k, distance, window, head):
+        past_keep, past_add, past_head, past_tail = parts(came[k])
+        past_tail = jnp.where(exists(distance), past_tail, -1.0)
+        joined = link(past_tail, head) * low(
+            jnp.concatenate([past_keep, past_add], axis=0), spread(window[:half], same_head)
+        )
+        return joined + jnp.concatenate([zeros, window[half:]], axis=0), past_head
+
+    keep_element(0, window, head, tail)
+    scan_copy(0).start()
 
     lane32, row32 = iota((count, count), 1), iota((count, count), 0)
     eye32 = lane32 == row32
@@ -374,37 +399,30 @@
     ).astype(F32)
     place[...] = table.T.astype(BF16)
     table = table.astype(BF16)
+    scan_copy(0).wait_recv()
+    window, head = doubled(0, 1, window, head)
+    keep_element(1, window, head, tail)
+    scan_copy(1).start()
     round_copy(0).wait_recv()
     round_copy(1).wait_recv()
     round_copy(2).start()
-    for k in range(1, REACH + 1):
-        near_copy(k).wait_recv()
-    keep, add, win_head, tail = parts(near[REACH - 1])
-    tail = jnp.where(exists(REACH), tail, -1.0)
-    for k in range(REACH - 1, 0, -1):
-        next_keep, next_add, next_head, next_tail = parts(near[k - 1])
-        step = link(tail, next_head) * low(
-            jnp.concatenate([keep, add], axis=0), spread(next_keep, same_head)
-        )
-        keep, add = step[:half], step[half:] + next_add
-        tail = jnp.where(exists(k), next_tail, -1.0)
-    window[...] = jnp.concatenate(
-        [add, jnp.broadcast_to(tail, (16, n))], axis=0
-    ).astype(BF16)
-    far_copy = pltpu.make_async_remote_copy(
-        src_ref=window, dst_ref=far, send_sem=far_sem.at[0], recv_sem=far_sem.at[1],
-        device_id={"sp": chip_peer(REACH)}, device_id_type=MESH,
-    )
-    far_copy.start()
-    for k in range(1, REACH + 1):
-        near_copy(k).wait_send()
+    scan_copy(1).wait_recv()
+    window, head = doubled(1, 2, window, head)
+    far[0] = jnp.concatenate([window[half:], jnp.broadcast_to(tail, (16, n))], axis=0).astype(BF16)
+    scan_copy(3).start()
+    keep_element(2, window, head, tail)
+    scan_copy(2).start()
     round_copy(2).wait_recv()
     for o in range(1, TP):
         give_copy(o).start()
-    far_copy.wait()
-    far_value = far[...].astype(F32)
-    far_tail = jnp.where(exists(REACH), far_value[half : half + 1], -1.0)
-    add = add + link(far_tail, win_head) * low(far_value[:half], spread(keep, same_head))
+    scan_copy(2).wait_recv()
+    keep, add, past_head, past_tail = parts(came[2])
+    keep = spread(keep, same_head)
+    scan_copy(3).wait_recv()
+    far_value = far[1].astype(F32)
+    far_tail = jnp.where(exists(REACH + 1), far_value[half : half + 1], -1.0)
+    add = add + link(far_tail, past_head) * low(far_value[:half], keep)
+    tail = jnp.where(exists(1), past_tail, -1.0)
     state = link(tail, own_head) * add
     passed = (low(state, spread(own_keep, same_head)) + own_add) * joined
     entering[0] = passed.astype(BF16)
@@ -522,14 +540,16 @@
     take(3)
     work(1)
     work(2)
+    work(3)
     give(1)
-    work(3)
     give(2)
     give(3)
     returned[size - piece :] = combined[size - piece :]
 
     for k in range(3):
         round_copy(k).wait_send()
+    for k in range(4):
+        scan_copy(k).wait_send()
     for o in range(1, TP):
         give_copy(o).wait_send()
         mix_copy(o).wait_send()
@@ -575,10 +595,9 @@
             scratch_shapes=[
                 pltpu.VMEM((2, n + 16, n), BF16),
                 pltpu.VMEM((n + 16, n), BF16),
-                pltpu.VMEM((n + 16, n), BF16),
-                pltpu.VMEM((REACH, n + 16, n), BF16),
-                pltpu.VMEM((n // 2 + 16, n), BF16),
-                pltpu.VMEM((n // 2 + 16, n), BF16),
+                pltpu.VMEM((4, n + 16, n), BF16),
+                pltpu.VMEM((3, n + 16, n), BF16),
+                pltpu.VMEM((2, n // 2 + 16, n), BF16),
                 pltpu.VMEM((2, n // 2, n), BF16),
                 pltpu.VMEM((TP, count, channels), BF16),
                 pltpu.VMEM((TP, count, channels), BF16),
@@ -600,7 +619,7 @@
                 pltpu.VMEM((width, hidden_units), BF16),
                 pltpu.VMEM((width, hidden_units), BF16),
                 pltpu.VMEM((hidden_units, width), BF16),
-                dma((4,)), dma((4,)), dma((REACH,)), dma((REACH,)), dma((2,)), dma((3,)), dma((3,)),
+                dma((4,)), dma((4,)), dma((4,)), dma((4,)), dma((3,)), dma((3,)),
                 dma((TP,)), dma((TP,)), dma((TP,)), dma((TP,)), dma((SP,)), dma((SP,)), dma((SP,)), dma((SP,)),
                 dma((CHUNKS * TP,)), dma((CHUNKS * TP,)), dma((CHUNKS * TP,)), dma((CHUNKS * TP,)),
                 dma((SP,)), dma((SP,)),

time: 111 us -> 110 us (level)
  no operation moved by 1% of the time
where the time goes in v4:
time: 110 us
  Pallas kernels  108 us (98%)
  local copies, waits for them, and re-layouts  1.57 us (1%)
    pallas_call x1, Pallas kernels, body(): pl.pallas_call(functools.partial(kernel, (SP, TP)), out_shape=jax.ShapeDt...  108 us

profile of v4, /device:TPU:33, one launch (start us, length us, event | category | flops | bytes accessed | tf_op | source)
XLA Modules:
  0.0 109.7 jit_solution(10530027901777638455)
XLA Ops:
  0.0 108.2 %shard_map.181 = bf16[32,2048]{1,0:T(8,128)(2,1)} custom-call(bf16[128,128]{1,0:T(8,128)(2,1)} %refs_0_.1, bf16[128,128]{1,0:T(8,128)(2,1)} %refs_1_.1, bf16[128,128]{1,0:T(8,128)(2,1)} %refs_2_.1, bf16[128,128]{1,0:T(8,128)(2,1)} %refs_3_.1, bf16[128,128]{1,0:T(8,128)(2,1)} %refs_4_.1, bf16[128,128]{1,0:T(8,128)(2,1)} %refs_5_.1, bf16[128,128]{1,0:T(8,128)(2,1)} %refs_6_.1, ...), custom_call_target="tpu_custom_call" | custom-call | tf_op jit(solution)/shard_map/pallas_call | solution.py:590
  108.2 1.6 %copy.21 = bf16[32,2048]{1,0:T(8,128)(2,1)} copy(bf16[32,2048]{1,0:T(8,128)(2,1)} %shard_map.181) | data formatting | bytes 262144

commit v5 on v4

--- a/solution.py
+++ b/solution.py
@@ -19,7 +19,7 @@
 SLOTS = 4
 GROUP = 4
 CAP = 2
-CHUNKS = 4
+CHUNKS = 8
 REACH = 4
 
 
@@ -536,14 +536,26 @@
     work(0)
     take(1)
     give(0)
+    work(1)
     take(2)
     take(3)
-    work(1)
+    give(1)
     work(2)
     work(3)
-    give(1)
+    take(4)
+    take(5)
     give(2)
     give(3)
+    work(4)
+    work(5)
+    take(6)
+    take(7)
+    give(4)
+    give(5)
+    work(6)
+    work(7)
+    give(6)
+    give(7)
     returned[size - piece :] = combined[size - piece :]
 
     for k in range(3):

time: 110 us -> 114 us (1.036)
  Pallas kernels: 108 us -> 112 us
    pallas_call x1, Pallas kernels: 108 us -> 112 us  [body(): pl.pallas_call(functools.partial(kernel, (SP, TP)), out_shape=jax.ShapeDt...]
where the time goes in v5:
time: 114 us
  Pallas kernels  112 us (98%)
  local copies, waits for them, and re-layouts  1.57 us (1%)
    pallas_call x1, Pallas kernels, body(): pl.pallas_call(functools.partial(kernel, (SP, TP)), out_shape=jax.ShapeDt...  112 us

profile of v5, /device:TPU:33, one launch (start us, length us, event | category | flops | bytes accessed | tf_op | source)
XLA Modules:
  0.0 113.6 jit_solution(4878667340840621136)
XLA Ops:
  0.0 112.1 %shard_map.181 = bf16[32,2048]{1,0:T(8,128)(2,1)} custom-call(bf16[128,128]{1,0:T(8,128)(2,1)} %refs_0_.1, bf16[128,128]{1,0:T(8,128)(2,1)} %refs_1_.1, bf16[128,128]{1,0:T(8,128)(2,1)} %refs_2_.1, bf16[128,128]{1,0:T(8,128)(2,1)} %refs_3_.1, bf16[128,128]{1,0:T(8,128)(2,1)} %refs_4_.1, bf16[128,128]{1,0:T(8,128)(2,1)} %refs_5_.1, bf16[128,128]{1,0:T(8,128)(2,1)} %refs_6_.1, ...), custom_call_target="tpu_custom_call" | custom-call | tf_op jit(solution)/shard_map/pallas_call | solution.py:602
  112.1 1.6 %copy.21 = bf16[32,2048]{1,0:T(8,128)(2,1)} copy(bf16[32,2048]{1,0:T(8,128)(2,1)} %shard_map.181) | data formatting | bytes 262144
